TPU v7x, 256 devices: a whole 4x4x8 slice. The times are simulated.
256 devices in a mesh: sp: 16 (over y, x), tp: 16 (over z, core).
Axes of the slice: x: 4, y: 4, z: 8, core: 2. Of those that a mesh axis runs over, the one named last changes fastest.
Arguments:
- cotangent: bfloat16 [4096, 2048], P('sp', 'tp'), may hold values from -6 to 6
- block_input: bfloat16 [4096, 2048], P('sp', 'tp'), may hold values from -6 to 6
- routes: int32 [4096, 2], P('sp'), may hold values from 0 to 15, all different within a row; in each aligned block of 256 rows (0 to 255, 256 to 511, ...) at most 40 rows name the same one
- route_weights: float32 [4096, 2], P('sp'), may hold values from 0.1 to 0.9
- gate_weight: bfloat16 [16, 2048, 7168], P('sp', None, 'tp'), may hold values from -0.125 to 0.125
- up_weight: bfloat16 [16, 2048, 7168], P('sp', None, 'tp'), may hold values from -0.125 to 0.125
- down_weight: bfloat16 [16, 7168, 2048], P('sp', 'tp'), may hold values from -0.0625 to 0.0625
- out_weight: bfloat16 [1024, 2048], P('tp'), may hold values from -0.1875 to 0.1875
- conv_out: bfloat16 [1024, 4096], P('tp', 'sp'), may hold values from -6 to 6
- gate_pre: bfloat16 [1024, 4096], P('tp', 'sp'), may hold values from -6 to 6
- prior_states: bfloat16 [1024, 4096], P('tp', 'sp'), may hold values from -6 to 6
- recur_weight: bfloat16 [16, 64, 64], replicated, may hold values from -0.75 to 0.75
- input_gate_matrix: bfloat16 [16, 64, 64], replicated, may hold values from -0.75 to 0.75
- decay_param: float32 [1024], replicated, may hold values from 4 to 16
- decay_jump: float32 [1024, 4096], P('tp', 'sp'), may hold values from -1 to 0, as said below
Outputs:
- gate_weight_grad: bfloat16 [16, 2048, 7168], P('sp', None, 'tp')
- up_weight_grad: bfloat16 [16, 2048, 7168], P('sp', None, 'tp')
- down_weight_grad: bfloat16 [16, 7168, 2048], P('sp', 'tp')
- out_weight_grad: float32 [1024, 2048], P('tp', 'sp')
- conv_grad: bfloat16 [1024, 4096], P('tp', 'sp')
- valve_logit_derivative: bfloat16 [1024, 4096], P('tp', 'sp')
Inputs may be any that keep to these rules, and one draw needn't show every extreme that they name: In each aligned block of 256 rows (the rows of one index of sp) no expert is named by more than 40 routes, a bound that some block reaches; a row names 2 different experts. `decay_jump`: every entry is at most -1 / 81920.
All inputs are finite; a program needn't handle non-finite values.
Results may differ from a plain program's by a relative error of at most 0.018.
Values may be sent and summed in bfloat16 or wider, within the bound.
A program may use at most 128 MiB of HBM per device.

v0:
```python
import jax
import jax.numpy as jnp
from jax import lax
from jax.sharding import Mesh
from jax.sharding import PartitionSpec as P

HEAD_DIM = 64
TOP_K = 2
TP = ("tp_0", "tp_1")


RATE_SCALE = 8.0


def side_by_side(arrays, axis, split_dim, concat_dim, along):
    widths = [a.shape[along] for a in arrays]
    both = jnp.concatenate(arrays, axis=along)
    whole = lax.all_to_all(both, axis, split_axis=split_dim, concat_axis=concat_dim, tiled=True)
    return tuple(jnp.split(whole, [sum(widths[:k]) for k in range(1, len(widths))], axis=along))


def side_by_side_2(arrays, axis, dim, along):
    both = jnp.concatenate(arrays, axis=along)
    whole, at, outs = (lax.all_gather(both, axis, axis=dim, tiled=True), 0, [])
    for a in arrays:
        outs.append(lax.slice_in_dim(whole, at, at + a.shape[along], axis=along))
        at += a.shape[along]
    return tuple(outs)


def in_blocks(value, dim, devices):
    before, after = (value.shape[:dim], value.shape[dim + 1 :])
    return jnp.moveaxis(value.reshape(*before, devices, -1, *after), dim, 0)


def scatter_pairs(value, chips, core, dim):
    sizes = (lax.axis_size(chips), lax.axis_size(core))
    tiles = in_blocks(value, dim, sizes[0] * sizes[1])
    inside = tiles.shape[1:]
    tiles = tiles.reshape(*sizes, *inside).swapaxes(0, 1).reshape(-1, *inside)
    tiles = lax.psum_scatter(tiles, core, scatter_dimension=0, tiled=True)
    return lax.psum_scatter(tiles, chips, scatter_dimension=0, tiled=True)[0]


def from_everyone(value, axis):
    devices = lax.axis_size(axis)
    return lax.all_to_all(
        jnp.broadcast_to(value[None], (devices, *value.shape)), axis, 0, 0, tiled=True
    )


def all_in_one(value, axis):
    leaves = jax.tree.leaves(value)
    sequence = sorted(range(len(leaves)), key=lambda k: -leaves[k].size)
    width = (1, *leaves[sequence[0]].shape)[-1]
    lines = [
        jnp.pad(leaves[k].reshape(-1), (0, -leaves[k].size % width)).reshape(-1, width)
        for k in sequence
    ]
    both, at, found = (from_everyone(jnp.concatenate(lines), axis), 0, {})
    for k, line in zip(sequence, lines):
        slab = both[:, at : at + len(line)].reshape(len(both), -1)
        found[k] = slab[:, : leaves[k].size].reshape(-1, *leaves[k].shape)
        at += len(line)
    numbers = iter(range(len(leaves)))
    return jax.tree.map(lambda _: found[next(numbers)], value)


def folded_in_pairs(pieces, combine):
    while len(jax.tree.leaves(pieces)[0]) > 1:
        pieces = jax.vmap(combine)(
            *(jax.tree.map(lambda part: part[side::2], pieces) for side in (0, 1))
        )
    return jax.tree.map(lambda part: part[0], pieces)


def prefix(value, axis, combine, identity):
    devices, place = (lax.axis_size(axis), lax.axis_index(axis))
    passed = jnp.arange(devices) > place

    def kept(part, zero, own):
        part = jnp.where(
            passed.reshape(-1, *(1 for _ in own.shape)), part, jnp.asarray(zero, own.dtype)
        )
        return part[::-1]

    pieces = all_in_one(value, axis)
    return folded_in_pairs(jax.tree.map(kept, pieces, identity, value), combine)


def summed_on_arrival(value, axis, dim):
    tiles = in_blocks(value, dim, lax.axis_size(axis))
    arrived = lax.all_to_all(tiles, axis, split_axis=0, concat_axis=0, tiled=True)
    return arrived.astype(jnp.float32).sum(axis=0)


def link_pairs(left_pair, right_pair):
    return (left_pair[0] * right_pair[0], right_pair[0] * left_pair[1] + right_pair[1])


def later_first(earlier_pair, later_pair):
    return (earlier_pair[0] * later_pair[0], later_pair[1] + later_pair[0] * earlier_pair[1])


def routing_tables(routes, experts, capacity):
    flat_routes = routes.reshape(-1)
    onehot = (flat_routes[:, None] == jnp.arange(experts, dtype=jnp.int32)[None, :]).astype(
        jnp.int32
    )
    slot_rank = jnp.sum((jnp.cumsum(onehot, axis=0) - onehot) * onehot, axis=1)
    target = (flat_routes * capacity + slot_rank).reshape(routes.shape[0], routes.shape[1])
    slot_ids = jnp.arange(experts * capacity, dtype=jnp.int32)
    return jnp.transpose(target)[:, None, :] == slot_ids[None, :, None]


def spread(placing, route_hits, rows_in, cot_in, route_weights):
    sent_rows = jnp.dot(placing, rows_in, preferred_element_type=jnp.float32).astype(jnp.bfloat16)
    scaled = (
        jnp.transpose(route_weights)[:, :, None] * cot_in.astype(jnp.float32)[None, :, :]
    ).astype(jnp.bfloat16)
    sent_cot = jnp.einsum(
        "kst,ktd->sd", route_hits, scaled, preferred_element_type=jnp.float32
    ).astype(jnp.bfloat16)
    return (sent_rows, sent_cot)


def expert_work(slot_rows, slot_cot, w_gate, w_up, w_down):
    minor = (((1,), (1,)), ((), ()))
    gate_act = jnp.dot(slot_rows, w_gate, preferred_element_type=jnp.float32)
    up_act = jnp.dot(slot_rows, w_up, preferred_element_type=jnp.float32)
    sigma_gate = jax.nn.sigmoid(gate_act)
    silu_val = gate_act * sigma_gate
    hidden = (silu_val * up_act).astype(jnp.bfloat16)
    d_hidden = lax.dot_general(slot_cot, w_down, minor, preferred_element_type=jnp.float32)
    d_gate = (d_hidden * up_act * sigma_gate * (1.0 + gate_act * (1.0 - sigma_gate))).astype(
        jnp.bfloat16
    )
    d_up = (d_hidden * silu_val).astype(jnp.bfloat16)
    width_part = lax.dot_general(d_gate, w_gate, minor, preferred_element_type=jnp.float32)
    width_part = width_part + lax.dot_general(d_up, w_up, minor, preferred_element_type=jnp.float32)
    return (hidden, d_gate, d_up, width_part)


def weight_grads(slot_rows, slot_cot, hidden, d_gate, d_up):
    major = (((0,), (0,)), ((), ()))
    gate_grad = lax.dot_general(
        slot_rows, d_gate, major, preferred_element_type=jnp.float32
    ).astype(jnp.bfloat16)
    up_grad = lax.dot_general(slot_rows, d_up, major, preferred_element_type=jnp.float32).astype(
        jnp.bfloat16
    )
    down_grad = lax.dot_general(hidden, slot_cot, major, preferred_element_type=jnp.float32).astype(
        jnp.bfloat16
    )
    return (gate_grad[None], up_grad[None], down_grad[None])


def local(
    cotangent,
    block_input,
    routes,
    route_weights,
    gate_weight,
    up_weight,
    down_weight,
    out_weight,
    conv_out,
    gate_pre,
    prior_states,
    recur_weight,
    input_gate_matrix,
    decay_param,
    decay_jump,
):
    experts = lax.axis_size("sp")
    tok_rows = cotangent.shape[0]
    capacity = 5 * tok_rows * TOP_K // (4 * experts)
    route_hits = routing_tables(routes, experts, capacity)
    placing = jnp.sum(route_hits.astype(jnp.int32), axis=0).astype(jnp.bfloat16)
    hit_table = route_hits.astype(jnp.bfloat16)
    sent_rows, sent_cot = spread(placing, hit_table, block_input, cotangent, route_weights)
    part_rows, portion_adjoint = side_by_side(
        (sent_rows.reshape(experts, capacity, -1), sent_cot.reshape(experts, capacity, -1)),
        "sp",
        0,
        0,
        1,
    )
    got_rows, got_cot = side_by_side_2((part_rows, portion_adjoint), TP, 2, 0)
    full_width = got_rows.shape[2]
    slot_rows = got_rows.reshape(-1, full_width)
    slot_cot = got_cot.reshape(-1, full_width)
    hidden, d_gate, d_up, width_part = expert_work(
        slot_rows, slot_cot, gate_weight[0], up_weight[0], down_weight[0]
    )
    gate_grad, up_grad, down_grad = weight_grads(slot_rows, slot_cot, hidden, d_gate, d_up)
    summed = (
        scatter_pairs(
            width_part.reshape(experts, capacity, full_width).astype(jnp.bfloat16),
            "tp_0",
            "tp_1",
            2,
        )
        .astype(jnp.float32)
        .astype(jnp.bfloat16)
    )
    handed_result = lax.all_to_all(summed, "sp", split_axis=0, concat_axis=0, tiled=True).reshape(
        experts * capacity, -1
    )
    moe_grad = lax.dot_general(
        placing, handed_result, (((0,), (0,)), ((), ())), preferred_element_type=jnp.float32
    )
    block_grad = (cotangent.astype(jnp.float32) + moe_grad).astype(jnp.bfloat16)
    full_grad = lax.all_gather(block_grad, TP, axis=1, tiled=True)
    channels = conv_out.shape[0]
    length = conv_out.shape[1]
    head_count = channels // HEAD_DIM
    head_start = lax.axis_index(TP) * head_count
    w_recur = lax.dynamic_slice_in_dim(recur_weight, head_start, head_count, 0)
    w_input = lax.dynamic_slice_in_dim(input_gate_matrix, head_start, head_count, 0)
    rate_parameter = lax.dynamic_slice_in_dim(decay_param, head_start * HEAD_DIM, channels, 0)[
        :, None
    ]
    shaped = conv_out.reshape(head_count, HEAD_DIM, length)
    recur_gate = jax.nn.sigmoid(
        jnp.einsum("hij,hit->hjt", w_recur, shaped, preferred_element_type=jnp.float32).reshape(
            channels, length
        )
    )
    input_gate = jax.nn.sigmoid(
        jnp.einsum("hij,hit->hjt", w_input, shaped, preferred_element_type=jnp.float32).reshape(
            channels, length
        )
    )
    softened = jax.nn.softplus(-rate_parameter)
    log_decay = -RATE_SCALE * recur_gate * softened + decay_jump
    decay_val = jnp.exp(log_decay)
    norm_scale = jnp.sqrt(-jnp.expm1(2.0 * log_decay))
    conv_vals = conv_out.astype(jnp.float32)
    prior_vals = prior_states.astype(jnp.float32)
    state = decay_val * prior_vals + norm_scale * input_gate * conv_vals
    gelu_val, gelu_pull = jax.vjp(jax.nn.gelu, gate_pre.astype(jnp.float32))
    mixed = (gelu_val * state).astype(jnp.bfloat16)
    d_mixed = lax.dot_general(
        out_weight, full_grad, (((1,), (1,)), ((), ())), preferred_element_type=jnp.float32
    )
    valve_logit_derivative = gelu_pull(d_mixed * state)[0].astype(jnp.bfloat16)
    d_state = d_mixed * gelu_val
    shifted = jnp.concatenate([decay_val[:, 1:], jnp.ones((channels, 1), jnp.float32)], axis=1)
    flipped = lax.associative_scan(link_pairs, (jnp.flip(shifted, 1), jnp.flip(d_state, 1)), axis=1)
    decay_prod = jnp.flip(flipped[0], 1)
    local_sum = jnp.flip(flipped[1], 1)
    summary = (decay_val[:, 0] * decay_prod[:, 0], decay_val[:, 0] * local_sum[:, 0])
    carried = prefix(
        summary,
        "sp",
        later_first,
        (jnp.ones((channels,), jnp.float32), jnp.zeros((channels,), jnp.float32)),
    )[1]
    state_grad = local_sum + decay_prod * carried[:, None]
    grad_log = (
        state_grad * prior_vals * decay_val
        - state_grad * input_gate * conv_vals * decay_val * decay_val / norm_scale
    )
    grad_recur = (grad_log * -RATE_SCALE * softened * recur_gate * (1.0 - recur_gate)).astype(
        jnp.bfloat16
    )
    grad_input = (state_grad * norm_scale * conv_vals * input_gate * (1.0 - input_gate)).astype(
        jnp.bfloat16
    )
    back_recur = jnp.einsum(
        "hij,hjt->hit",
        w_recur,
        grad_recur.reshape(head_count, HEAD_DIM, length),
        preferred_element_type=jnp.float32,
    ).reshape(channels, length)
    back_input = jnp.einsum(
        "hij,hjt->hit",
        w_input,
        grad_input.reshape(head_count, HEAD_DIM, length),
        preferred_element_type=jnp.float32,
    ).reshape(channels, length)
    conv_grad = (state_grad * norm_scale * input_gate + back_recur + back_input).astype(
        jnp.bfloat16
    )
    projected = summed_on_arrival(
        lax.dot_general(
            full_grad, mixed, (((0,), (1,)), ((), ())), preferred_element_type=jnp.float32
        ).astype(jnp.bfloat16),
        "sp",
        0,
    )
    out_weight_grad = jnp.transpose(projected)
    return (gate_grad, up_grad, down_grad, out_weight_grad, conv_grad, valve_logit_derivative)


def solution(mesh):
    split = Mesh(mesh.devices.reshape(mesh.shape["sp"], 8, 2), ("sp", "tp_0", "tp_1"))
    return jax.shard_map(
        local,
        mesh=split,
        in_specs=(
            P("sp", TP),
            P("sp", TP),
            P("sp", None),
            P("sp", None),
            P("sp", None, TP),
            P("sp", None, TP),
            P("sp", TP, None),
            P(TP, None),
            P(TP, "sp"),
            P(TP, "sp"),
            P(TP, "sp"),
            P(),
            P(),
            P(),
            P(TP, "sp"),
        ),
        out_specs=(
            P("sp", None, TP),
            P("sp", None, TP),
            P("sp", TP, None),
            P(TP, "sp"),
            P(TP, "sp"),
            P(TP, "sp"),
        ),
        check_vma=False,
    )
```

profile of v0, /device:TPU:1, one launch (start us, length us, event | category | flops | bytes accessed | tf_op | source)
XLA Modules:
  0.0 276.3 jit_solution(1646220735173862300)
XLA Ops:
  13.5 15.9 %all_to_all.20 = bf16[16,80,128]{2,1,0:T(8,128)(2,1)S(1)} all-to-all(bf16[16,80,128]{2,1,0:T(8,128)(2,1)S(1)} %pad_maximum_fusion), channel_id=1, replica_groups=mesh['sp'=16,'tp_0'=8,'tp_1'=2] {'sp'}, dimensions={0} | all-to-all | bytes 655360 | tf_op jit(solution)/shard_map/all_to_all | solution.py:18
  30.2 54.1 %all-gather.3.cloned.1.call-done = bf16[32,40,2048]{2,1,0:T(8,128)(2,1)} async-done(((bf16[32,40,128]{2,1,0:T(8,128)(2,1)}), bf16[32,40,2048]{2,1,0:T(8,128)(2,1)}) %all-gather.3.cloned.1.call-update) | async-done | bytes 5242896 | tf_op jit(solution)/shard_map/all_gather | solution.py:24
  84.3 3.2 %fusion.103 = (bf16[16,40,2048]{2,1,0:T(8,128)(2,1)S(1)}, bf16[16,40,2048]{2,1,0:T(8,128)(2,1)S(1)}) fusion(bf16[32,40,2048]{2,1,0:T(8,128)(2,1)} %all-gather.3.cloned.1.call-done), kind=kLoop, calls=%fused_computation.190 | loop fusion | bytes 10485760 | tf_op jit(solution)/shard_map/slice | solution.py:26
  87.5 1.6 fusion.5
  89.2 1.2 copy-done.6
  90.4 1.6 fusion.8
  92.3 2.0 multiply_convert_fusion.1
  94.4 1.6 fusion.3
  95.9 1.6 fusion.12
  99.0 1.9 copy.84
  101.0 14.5 %reduce-scatter.3.cloned.1.call-done = bf16[8,16,40,128]{3,2,1,0:T(8,128)(2,1)} async-done(((bf16[16,16,40,128]{3,2,1,0:T(8,128)(2,1)}), bf16[8,16,40,128]{3,2,1,0:T(8,128)(2,1)}) %reduce-scatter.3.cloned.1.call-update) | async-done | bytes 1310736 | tf_op jit(solution)/shard_map/reduce_scatter | solution.py:41
  115.6 39.3 %reduce-scatter.5.cloned.1.call-done = bf16[1,16,40,128]{3,2,1,0:T(8,128)(2,1)} async-done(((bf16[8,16,40,128]{3,2,1,0:T(8,128)(2,1)}), bf16[1,16,40,128]{3,2,1,0:T(8,128)(2,1)}) %reduce-scatter.5.cloned.1.call-update) | async-done | bytes 163856 | tf_op jit(solution)/shard_map/reduce_scatter | solution.py:42
  154.9 13.5 %all_to_all.21 = bf16[16,40,128]{2,1,0:T(8,128)(2,1)S(1)} all-to-all(bf16[16,40,128]{2,1,0:T(8,128)(2,1)} %bitcast.140), channel_id=1, replica_groups=mesh['sp'=16,'tp_0'=8,'tp_1'=2] {'sp'}, dimensions={0} | all-to-all | bytes 327680 | tf_op jit(solution)/shard_map/all_to_all | solution.py:207
  172.0 4.9 %fusion.1 = bf16[1,2048,448]{1,2,0:T(8,128)(2,1)} fusion(bf16[640,448]{0,1:T(8,128)(2,1)} %copy-done.18, bf16[640,2048]{1,0:T(8,128)(2,1)} %bitcast.125), kind=kOutput, calls=%fused_computation.5 | convolution fusion | flops 1175322624 | bytes 5029888 | tf_op jit(solution)/shard_map/dot_general | solution.py:146
  176.9 2.9 %fusion.2 = bf16[1,2048,448]{1,2,0:T(8,128)(2,1)} fusion(bf16[640,448]{0,1:T(8,128)(2,1)S(1)} %get-tuple-element.12, bf16[640,2048]{1,0:T(8,128)(2,1)S(1)} %bitcast.126), kind=kOutput, calls=%fused_computation.6 | convolution fusion | flops 1175322624 | bytes 5029888 | tf_op jit(solution)/shard_map/dot_general | solution.py:149
  179.8 2.8 %fusion = bf16[1,448,2048]{2,1,0:T(8,128)(2,1)} fusion(bf16[640,2048]{1,0:T(8,128)(2,1)S(1)} %bitcast.122, f32[640,448]{0,1:T(8,128)S(1)} %copy-done.22, f32[640,448]{0,1:T(8,128)S(1)} %copy-done.20), kind=kOutput, calls=%fused_computation.4 | convolution fusion | flops 1177042944 | bytes 6750208 | tf_op jit(solution)/shard_map/dot_general | solution.py:152
  182.6 25.2 %all-gather.5.cloned.1.call-done = bf16[256,2048]{1,0:T(8,128)(2,1)} async-done(((bf16[256,128]{1,0:T(8,128)(2,1)}), bf16[256,2048]{1,0:T(8,128)(2,1)}) %all-gather.5.cloned.1.call-update) | async-done | bytes 1048592 | tf_op jit(solution)/shard_map/all_gather | solution.py:214
  207.9 2.3 fusion.44
  227.9 1.4 slice.409
  245.0 6.5 %all-to-all-start.3 = ((f32[16,1,128]{2,1,0:T(1,128)}), f32[16,1,128]{2,1,0:T(1,128)S(1)}, u32[]{:S(2)}, u32[]{:S(2)}) async-start(f32[16,1,128]{2,1,0:T(1,128)} %reshape.173), calls=%async_computation.5 | async-start | bytes 16384 | tf_op jit(solution)/shard_map/all_to_all | solution.py:47
  253.8 4.1 %all-to-all-done.3 = f32[16,1,128]{2,1,0:T(1,128)S(1)} async-done(((f32[16,1,128]{2,1,0:T(1,128)}), f32[16,1,128]{2,1,0:T(1,128)S(1)}, u32[]{:S(2)}, u32[]{:S(2)}) %all-to-all-start.3) | async-done | bytes 8224 | tf_op jit(solution)/shard_map/all_to_all | solution.py:47
  257.9 3.5 %all-to-all-start.2 = ((bf16[16,128,64]{1,2,0:T(8,128)(2,1)}), bf16[16,128,64]{1,2,0:T(8,128)(2,1)S(1)}, u32[]{:S(2)}, u32[]{:S(2)}) async-start(bf16[16,128,64]{1,2,0:T(8,128)(2,1)} %bitcast.107), calls=%async_computation.4 | async-start | bytes 524288 | tf_op jit(solution)/shard_map/all_to_all | solution.py:93
  264.1 1.5 fusion.27
  265.7 3.4 %all-to-all-done.2 = bf16[16,128,64]{1,2,0:T(8,128)(2,1)S(1)} async-done(((bf16[16,128,64]{1,2,0:T(8,128)(2,1)}), bf16[16,128,64]{1,2,0:T(8,128)(2,1)S(1)}, u32[]{:S(2)}, u32[]{:S(2)}) %all-to-all-start.2) | async-done | bytes 262176 | tf_op jit(solution)/shard_map/all_to_all | solution.py:93
  (234 shorter events, 50.9 us)
Async XLA Ops:
  7.2 80.4 %copy-start = (bf16[1,2048,448]{1,2,0:T(8,128)(2,1)S(1)}, bf16[1,2048,448]{1,2,0:T(8,128)(2,1)}, u32[]{:S(2)}) copy-start(bf16[1,2048,448]{1,2,0:T(8,128)(2,1)} %param.19) | copy-start | bytes 5505028
  7.2 6.0 %copy-start.13 = (bf16[256,128]{1,0:T(8,128)(2,1)S(1)}, bf16[256,128]{1,0:T(8,128)(2,1)}, u32[]{:S(2)}) copy-start(bf16[256,128]{1,0:T(8,128)(2,1)} %param.16) | copy-start | bytes 196612
  7.2 77.1 %all-gather.3.cloned.1.call-start = ((), (), s32[]{:S(2)}) async-start(), calls=%async_computation.6 | async-start | bytes 5570560 | tf_op jit(solution)/shard_map/all_gather | solution.py:24
  30.2 85.3 %reduce-scatter.3.cloned.1.call-start = ((), (), s32[]{:S(2)}) async-start(), calls=%async_computation.7 | async-start | bytes 3932160 | tf_op jit(solution)/shard_map/reduce_scatter | solution.py:41
  87.5 4.6 %copy-start.2 = (bf16[16,40,2048]{2,1,0:T(8,128)(2,1)}, bf16[16,40,2048]{2,1,0:T(8,128)(2,1)S(1)}, u32[]{:S(2)}) copy-start(bf16[16,40,2048]{2,1,0:T(8,128)(2,1)S(1)} %get-tuple-element.10) | copy-start | bytes 7864324
  87.5 2.9 %copy-start.6 = (bf16[1,2048,448]{1,2,0:T(8,128)(2,1)S(1)}, bf16[1,2048,448]{1,2,0:T(8,128)(2,1)}, u32[]{:S(2)}) copy-start(bf16[1,2048,448]{1,2,0:T(8,128)(2,1)} %param.20) | copy-start | bytes 5505028
  100.9 67.4 %copy-start.9 = (bf16[256,128]{1,0:T(8,128)(2,1)S(1)}, bf16[256,128]{1,0:T(8,128)(2,1)}, u32[]{:S(2)}) copy-start(bf16[256,128]{1,0:T(8,128)(2,1)} %param.15) | copy-start | bytes 196612
  101.0 69.2 %copy-start.7 = (bf16[64,256]{1,0:T(8,128)(2,1)S(1)}, bf16[64,256]{1,0:T(8,128)(2,1)}, u32[]{:S(2)}) copy-start(bf16[64,256]{1,0:T(8,128)(2,1)} %param.23) | copy-start | bytes 98308
  101.0 53.9 %reduce-scatter.5.cloned.1.call-start = ((), (), s32[]{:S(2)}) async-start(), calls=%async_computation.8 | async-start | bytes 1474560 | tf_op jit(solution)/shard_map/reduce_scatter | solution.py:42
  115.5 92.3 %all-gather.5.cloned.1.call-start = ((), (), s32[]{:S(2)}) async-start(), calls=%async_computation.9 | async-start | bytes 1114112 | tf_op jit(solution)/shard_map/all_gather | solution.py:214
  172.0 35.9 %copy-start.15 = (f32[64,256]{1,0:T(8,128)}, f32[64,256]{1,0:T(8,128)S(1)}, u32[]{:S(2)}) copy-start(f32[64,256]{1,0:T(8,128)S(1)} %fusion.26) | copy-start | bytes 196612
  172.0 4.9 %copy-start.5 = (bf16[16,40,2048]{2,1,0:T(8,128)(2,1)S(1)}, bf16[16,40,2048]{2,1,0:T(8,128)(2,1)}, u32[]{:S(2)}) copy-start(bf16[16,40,2048]{2,1,0:T(8,128)(2,1)} %copy-done.4) | copy-start | bytes 7864324
  176.9 2.9 %copy-start.3 = (bf16[16,40,2048]{2,1,0:T(8,128)(2,1)S(1)}, bf16[16,40,2048]{2,1,0:T(8,128)(2,1)}, u32[]{:S(2)}) copy-start(bf16[16,40,2048]{2,1,0:T(8,128)(2,1)} %copy-done.2) | copy-start | bytes 7864324
  176.9 2.9 %copy-start.20 = (f32[640,448]{0,1:T(8,128)S(1)}, f32[640,448]{0,1:T(8,128)}, u32[]{:S(2)}) copy-start(f32[640,448]{0,1:T(8,128)} %copy-done.19) | copy-start | bytes 3440644
  176.9 2.9 %copy-start.22 = (f32[640,448]{0,1:T(8,128)S(1)}, f32[640,448]{0,1:T(8,128)}, u32[]{:S(2)}) copy-start(f32[640,448]{0,1:T(8,128)} %copy-done.21) | copy-start | bytes 3440644
  179.7 28.1 %copy-start.8 = (bf16[64,2048]{1,0:T(8,128)(2,1)S(1)}, bf16[64,2048]{1,0:T(8,128)(2,1)}, u32[]{:S(2)}) copy-start(bf16[64,2048]{1,0:T(8,128)(2,1)} %param.22) | copy-start | bytes 786436
  179.8 28.1 %copy-start.10 = (bf16[64,256]{1,0:T(8,128)(2,1)S(1)}, bf16[64,256]{1,0:T(8,128)(2,1)}, u32[]{:S(2)}) copy-start(bf16[64,256]{1,0:T(8,128)(2,1)} %param.24) | copy-start | bytes 98308
  179.8 28.1 %copy-start.11 = (bf16[64,256]{1,0:T(8,128)(2,1)S(1)}, bf16[64,256]{1,0:T(8,128)(2,1)}, u32[]{:S(2)}) copy-start(bf16[64,256]{1,0:T(8,128)(2,1)} %param.25) | copy-start | bytes 98308
  179.8 28.1 %copy-start.14 = (f32[64,256]{1,0:T(8,128)S(1)}, f32[64,256]{1,0:T(8,128)}, u32[]{:S(2)}) copy-start(f32[64,256]{1,0:T(8,128)} %param.29) | copy-start | bytes 196612
  232.0 19.6 %copy-start.1 = (bf16[256,2048]{1,0:T(8,128)(2,1)S(1)}, bf16[256,2048]{1,0:T(8,128)(2,1)}, u32[]{:S(2)}) copy-start(bf16[256,2048]{1,0:T(8,128)(2,1)} %all-gather.5.cloned.1.call-done) | copy-start | bytes 3145732
  244.1 19.1 %copy-start.12 = (bf16[64,256]{1,0:T(8,128)(2,1)S(1)}, bf16[64,256]{1,0:T(8,128)(2,1)}, u32[]{:S(2)}) copy-start(bf16[64,256]{1,0:T(8,128)(2,1)} %param.25) | copy-start | bytes 98308
  244.1 19.0 %copy-start.16 = (f32[64,256]{1,0:T(8,128)S(1)}, f32[64,256]{1,0:T(8,128)}, u32[]{:S(2)}) copy-start(f32[64,256]{1,0:T(8,128)} %copy-done.15) | copy-start | bytes 196612
  245.0 12.9 %all-to-all-start.3 = ((f32[16,1,128]{2,1,0:T(1,128)}), f32[16,1,128]{2,1,0:T(1,128)S(1)}, u32[]{:S(2)}, u32[]{:S(2)}) async-start(f32[16,1,128]{2,1,0:T(1,128)} %reshape.173), calls=%async_computation.5 | async-start | bytes 16384 | tf_op jit(solution)/shard_map/all_to_all | solution.py:47
  257.9 11.2 %all-to-all-start.2 = ((bf16[16,128,64]{1,2,0:T(8,128)(2,1)}), bf16[16,128,64]{1,2,0:T(8,128)(2,1)S(1)}, u32[]{:S(2)}, u32[]{:S(2)}) async-start(bf16[16,128,64]{1,2,0:T(8,128)(2,1)} %bitcast.107), calls=%async_computation.4 | async-start | bytes 524288 | tf_op jit(solution)/shard_map/all_to_all | solution.py:93
  (5 other events, 9.1 us)
Sparse Core Ops, SparseCore 0:
  30.3 53.9 all-gather.2
  101.1 14.3 reduce-scatter.2
  118.1 36.7 reduce-scatter.4
  169.4 38.4 all-gather.4
where the time goes:
time: 278 us; the launch traced here: 276 us
  waiting for transfers between devices  141 us (51%)
  local copies, waits for them, and re-layouts  42 us (15%)
  blocking collectives  29.4 us (11%)
  matrix products  29 us (10%)
  between operations  14.8 us (5%)
  starting transfers between devices  10.2 us (4%)
  other arithmetic  10.1 us (4%)
    all_gather x1, waiting for transfers between devices, side_by_side_2(): whole, at, outs = (lax.all_gather(both, axis, axis=dim, tiled=True), 0, [])  54.1 us
    reduce_scatter x1, waiting for transfers between devices, scatter_pairs(): return lax.psum_scatter(tiles, chips, scatter_dimension=0, tiled=True)[0]  39.3 us
    all_gather x1, waiting for transfers between devices, local(): full_grad = lax.all_gather(block_grad, TP, axis=1, tiled=True)  25.2 us
    slice x47, local copies, waits for them, and re-layouts, local(): lax.associative_scan(link_pairs, (jnp.flip(shifted, 1), jnp.flip(d_state,...  19.1 us
    all_to_all x1, blocking collectives, side_by_side(): lax.all_to_all(both, axis, split_axis=split_dim, concat_axis=concat_dim,...  15.9 us
    reduce_scatter x1, waiting for transfers between devices, scatter_pairs(): tiles = lax.psum_scatter(tiles, core, scatter_dimension=0, tiled=True)  14.5 us
    all_to_all x1, blocking collectives, local(): lax.all_to_all(summed, 'sp', split_axis=0, concat_axis=0, tiled=True)  13.5 us
    pad x28, local copies, waits for them, and re-layouts, local(): lax.associative_scan(link_pairs, (jnp.flip(shifted, 1), jnp.flip(d_state,...  10.2 us
  transfers between devices with their start and end apart: 6, of which 6 were waited for; matrix products, arithmetic and copies ran while one was open for 7% of the time, Pallas kernels for 0%

commit v1 on v0

v1 whole, which is shorter than its diff:
```python
import functools

import jax
import jax.numpy as jnp
from jax import lax
from jax.experimental import pallas as pl
from jax.experimental.pallas import tpu as pltpu
from jax.sharding import Mesh
from jax.sharding import PartitionSpec as P

F32 = jnp.float32
BF16 = jnp.bfloat16
MESH = pl.DeviceIdType.MESH

NY, NX, NZ, NC = 4, 4, 8, 2
NSP = NY * NX
NTP = NZ * NC
HEAD_DIM = 64
CAP = 40
TOK = 256
SLOTS = NSP * CAP
HALF = SLOTS // 2
COL = 128
FFD = 448
RATE_SCALE = 8.0
GELU_A = 0.7978845608028654
GELU_B = 0.044715
REACH = ((NZ // 2, NZ // 2 - 1), (NZ // 2 - 1, NZ // 2))

NT = (((1,), (1,)), ((), ()))
TN = (((0,), (0,)), ((), ()))


def dot(a, b):
    return jnp.dot(a, b, preferred_element_type=F32)


def dot_nt(a, b):
    return lax.dot_general(a, b, NT, preferred_element_type=F32)


def dot_tn(a, b):
    return lax.dot_general(a, b, TN, preferred_element_type=F32)


def minus_expm1(v):
    series = jnp.full_like(v, 1.0)
    for k in range(10, 1, -1):
        series = 1.0 + series * v * (1.0 / k)
    return jnp.where(v > -0.5, -v * series, 1.0 - jnp.exp(v))


def remote(src, dst, send, recv, where):
    return pltpu.make_async_remote_copy(
        src_ref=src, dst_ref=dst, send_sem=send, recv_sem=recv, device_id=where, device_id_type=MESH
    )


def main_kernel(
    routes_ref,
    weights_ref,
    rows_ref,
    cot_ref,
    decay_ref,
    gate_hbm,
    up_hbm,
    down_hbm,
    out_w_hbm,
    conv_hbm,
    pre_hbm,
    prior_hbm,
    jump_hbm,
    recur_hbm,
    input_hbm,
    gathered_hbm,
    acts_hbm,
    out_grad_ref,
    conv_grad_ref,
    valve_ref,
    wg,
    wu,
    wd,
    ow,
    conv_v,
    pre_v,
    prior_v,
    jump_v,
    wr,
    wi,
    sent,
    ag,
    acc_g,
    acc_u,
    acc_d,
    acts,
    own,
    pstage,
    precv,
    ring_out,
    ring_in,
    sums,
    back,
    fg,
    summary,
    summaries,
    ow_out,
    ow_in,
    load_sem,
    a2a_send,
    a2a_recv,
    a2a_self,
    ag_send,
    ag_recv,
    agp_send,
    agp_recv,
    store_sem,
    rp_send,
    rp_recv,
    rr_send,
    rr_recv,
    back_send,
    back_recv,
    back_self,
    fg_send,
    fg_recv,
    fgp_send,
    fgp_recv,
    sum_send,
    sum_recv,
    ow_send,
    ow_recv,
):
    y, x, z, c = (lax.axis_index(n) for n in ("y", "x", "z", "core"))
    s = y * NX + x
    tp = z * NC + c
    mate = {"core": 1 - c}

    def peer(i):
        q = lax.rem(s + i, NSP)
        return q, {"y": q // NX, "x": lax.rem(q, NX)}

    def z_at(o):
        return lax.rem(z + o + 2 * NZ, NZ)

    beside = ({"z": z_at(1)}, {"z": z_at(-1)})

    loads = [
        pltpu.make_async_copy(a, b, load_sem.at[i])
        for i, (a, b) in enumerate(
            (
                (gate_hbm.at[0], wg),
                (up_hbm.at[0], wu),
                (down_hbm.at[0], wd),
                (conv_hbm, conv_v),
                (pre_hbm, pre_v),
                (prior_hbm, prior_v),
                (jump_hbm, jump_v),
                (recur_hbm, wr),
                (input_hbm, wi),
                (out_w_hbm, ow),
            )
        )
    ]
    for load in loads:
        load.start()

    barrier = pltpu.get_barrier_semaphore()
    for i in range(1, NSP):
        pl.semaphore_signal(barrier, inc=1, device_id=peer(i)[1], device_id_type=MESH)
    for where in (*beside, mate):
        pl.semaphore_signal(barrier, inc=1, device_id=where, device_id_type=MESH)

    expert_lane = lax.broadcasted_iota(jnp.int32, (TOK, NSP), 1)
    hot = [(expert_lane == routes_ref[:, k : k + 1]).astype(F32) for k in range(2)]
    tok_sub = lax.broadcasted_iota(jnp.int32, (TOK, TOK), 0)
    tok_lane = lax.broadcasted_iota(jnp.int32, (TOK, TOK), 1)
    earlier = (tok_lane < tok_sub).astype(BF16)
    before = dot(earlier, (hot[0] + hot[1]).astype(BF16))
    targets = [
        jnp.sum(hot[k] * before, axis=1, keepdims=True).astype(jnp.int32)
        + routes_ref[:, k : k + 1] * CAP
        for k in range(2)
    ]
    slot_sub = lax.broadcasted_iota(jnp.int32, (SLOTS, TOK), 0)
    across = [
        jnp.sum(jnp.where(tok_sub == tok_lane, t, 0), axis=0, keepdims=True) for t in targets
    ]
    hits = [(slot_sub == t).astype(F32) for t in across]
    placing = (hits[0] + hits[1]).astype(BF16)
    sent[0] = dot(placing, rows_ref[...]).astype(BF16)
    cot = cot_ref[...].astype(F32)
    sent_cot = dot(hits[0].astype(BF16), (weights_ref[:, 0:1] * cot).astype(BF16)) + dot(
        hits[1].astype(BF16), (weights_ref[:, 1:2] * cot).astype(BF16)
    )
    sent[1] = sent_cot.astype(BF16)

    pl.semaphore_wait(barrier, NSP - 1 + 3)

    def a2a(i, a):
        q, where = peer(i)
        return remote(
            sent.at[a, pl.ds(pl.multiple_of(q * CAP, 8), CAP)],
            ag.at[tp, a, pl.ds(pl.multiple_of(s * CAP, 8), CAP)],
            a2a_send.at[a, i],
            a2a_recv.at[a, i],
            where,
        )

    selfs = []
    for a in range(2):
        for i in range(1, NSP):
            a2a(i, a).start()
        mine = pl.ds(pl.multiple_of(s * CAP, 8), CAP)
        selfs.append(pltpu.make_async_copy(sent.at[a, mine], ag.at[tp, a, mine], a2a_self.at[a]))
        selfs[-1].start()

    def ag_hop(d, k, a):
        o = -k if d == 0 else k
        ref = ag.at[z_at(o) * NC + c, a]
        return remote(ref, ref, ag_send.at[d, k, a], ag_recv.at[d, k, a], beside[d])

    def ag_mate(o, a):
        ref = ag.at[z_at(o) * NC + c, a]
        return remote(ref, ref, agp_send.at[o % NZ, a], agp_recv.at[o % NZ, a], mate)

    loads[0].wait()
    loads[1].wait()
    loads[2].wait()

    for a in range(2):
        for i in range(1, NSP):
            a2a(i, a).wait_recv()
        selfs[a].wait()
        ag_hop(0, 0, a).start()
        ag_hop(1, 0, a).start()
        ag_mate(0, a).start()

    def accumulate(o, first=False):
        for a in range(2):
            ag_mate(o, a).wait_recv()
        zc = z_at(o)
        cols = pl.ds(pl.multiple_of(zc * 2 * COL, 2 * COL), 2 * COL)

        def block(m, _):
            r = pl.ds(pl.multiple_of(m * HALF, HALF), HALF)
            xs = jnp.concatenate([ag[zc * NC, 0, r], ag[zc * NC + 1, 0, r]], axis=1)
            cs = jnp.concatenate([ag[zc * NC, 1, r], ag[zc * NC + 1, 1, r]], axis=1)
            g = dot(xs, wg[cols, :])
            u = dot(xs, wu[cols, :])
            h = dot_nt(cs, wd[:, cols])
            if first:
                acc_g[r, :] = g
                acc_u[r, :] = u
                acc_d[r, :] = h
            else:
                acc_g[r, :] += g
                acc_u[r, :] += u
                acc_d[r, :] += h
            return 0

        lax.fori_loop(0, 2, block, 0)

    for k in range(1, NZ // 2 + 1):
        for a in range(2):
            for d in range(2):
                if k <= REACH[d][a]:
                    ag_hop(d, k - 1, a).wait_recv()
                    if k < REACH[d][a]:
                        ag_hop(d, k, a).start()
                    ag_mate(-k if d == 0 else k, a).start()
        if k == 1:
            accumulate(0, True)
        else:
            accumulate(1 - k)
            accumulate(k - 1)
    accumulate(NZ // 2)

    store = pltpu.make_async_copy(ag, gathered_hbm, store_sem.at[0])
    store.start()

    def act(m, _):
        r = pl.ds(pl.multiple_of(m * 80, 80), 80)
        g = acc_g[r, :]
        u = acc_u[r, :]
        dh = acc_d[r, :]
        sig = jax.nn.sigmoid(g)
        silu = g * sig
        acts[0, r, :] = (silu * u).astype(BF16)
        acts[1, r, :] = (dh * u * sig * (1.0 + g * (1.0 - sig))).astype(BF16)
        acts[2, r, :] = (dh * silu).astype(BF16)
        return 0

    lax.fori_loop(0, SLOTS // 80, act, 0)
    store_acts = pltpu.make_async_copy(acts, acts_hbm, store_sem.at[1])
    store_acts.start()

    def pair_copy(o, a):
        r = pl.ds(a * HALF, HALF)
        return remote(pstage.at[o, r], precv.at[o, r], rp_send.at[o, a], rp_recv.at[o, a], mate)

    def width(o):
        cols = pl.ds(pl.multiple_of(z_at(o) * 2 * COL, 2 * COL), 2 * COL)
        for a in range(2):
            r = pl.ds(a * HALF, HALF)
            part = dot_nt(acts[1, r, :], wg[cols, :]) + dot_nt(acts[2, r, :], wu[cols, :])
            low, high = part[:, :COL], part[:, COL:]
            own[o, r, :] = jnp.where(c == 0, low, high)
            pstage[o, r, :] = jnp.where(c == 0, high, low).astype(BF16)
            pair_copy(o, a).start()

    def paired(o, a):
        pair_copy(o, a).wait_recv()
        r = pl.ds(a * HALF, HALF)
        return own[o, r, :] + precv[o, r, :].astype(F32)

    def rs_hop(d, j, a):
        return remote(
            ring_out.at[d, j, a], ring_in.at[d, j, a], rr_send.at[d, j, a], rr_recv.at[d, j, a], beside[d]
        )

    def rs_step(d, j, a):
        reach = REACH[d][a]
        if j >= reach:
            return
        o = (reach - j) if d == 0 else (j - reach)
        value = paired(o % NZ, a)
        if j > 0:
            rs_hop(d, j - 1, a).wait_recv()
            value = value + ring_in[d, j - 1, a].astype(F32)
        ring_out[d, j, a] = value.astype(BF16)
        rs_hop(d, j, a).start()

    half_way = NZ // 2
    width(half_way)
    width(half_way - 1)
    width(half_way + 1)
    for j in range(half_way):
        rs_step(0, j, 0)
        rs_step(1, j, 1)
        rs_step(0, j, 1)
        rs_step(1, j, 0)
        if j < half_way - 2:
            width(half_way - 2 - j)
            width(half_way + 2 + j)
        if j == half_way - 2:
            width(0)
    for a in range(2):
        r = pl.ds(a * HALF, HALF)
        value = paired(0, a)
        for d in range(2):
            last = REACH[d][a] - 1
            rs_hop(d, last, a).wait_recv()
            value = value + ring_in[d, last, a].astype(F32)
        sums[r, :] = value.astype(BF16)

    def give(i):
        q, where = peer(i)
        return remote(
            sums.at[pl.ds(pl.multiple_of(q * CAP, 8), CAP)],
            back.at[pl.ds(pl.multiple_of(s * CAP, 8), CAP)],
            back_send.at[i],
            back_recv.at[i],
            where,
        )

    for i in range(1, NSP):
        give(i).start()
    mine = pl.ds(pl.multiple_of(s * CAP, 8), CAP)
    keep = pltpu.make_async_copy(sums.at[mine], back.at[mine], back_self.at[0])
    keep.start()

    for load in loads[3:]:
        load.wait()
    sub = lax.broadcasted_iota(jnp.int32, (HEAD_DIM, 2 * HEAD_DIM), 0)
    lane = lax.broadcasted_iota(jnp.int32, (HEAD_DIM, 2 * HEAD_DIM), 1)
    first_lane = lax.rem(tp, 2) * HEAD_DIM
    decay_row = decay_ref[pl.ds(tp // 2, 1), :]
    rate = jnp.sum(jnp.where(lane == sub + first_lane, decay_row, 0.0), axis=1, keepdims=True)
    softened = jnp.maximum(-rate, 0.0) + jnp.log1p(jnp.exp(-jnp.abs(rate)))
    conv_b = conv_v[...]
    conv = conv_b.astype(F32)
    w_recur = wr[tp]
    w_input = wi[tp]
    recur_gate = jax.nn.sigmoid(dot_tn(w_recur, conv_b))
    input_gate = jax.nn.sigmoid(dot_tn(w_input, conv_b))
    log_decay = -RATE_SCALE * recur_gate * softened + jump_v[...]
    decay = jnp.exp(log_decay)
    norm = jnp.sqrt(minus_expm1(2.0 * log_decay))
    prior = prior_v[...].astype(F32)
    state = decay * prior + norm * input_gate * conv
    pre = pre_v[...].astype(F32)
    squared = pre * pre
    t = jnp.tanh(GELU_A * (pre + GELU_B * pre * squared))
    gelu = pre * (0.5 * (1.0 + t))
    d_gelu = 0.5 * (1.0 + t) + 0.5 * pre * (1.0 - t * t) * GELU_A * (1.0 + 3.0 * GELU_B * squared)
    mixed = (gelu * state).astype(BF16)
    time = lax.broadcasted_iota(jnp.int32, (HEAD_DIM, TOK), 1)
    scan_a = [jnp.where(time == TOK - 1, 1.0, pltpu.roll(decay, TOK - 1, 1))]
    reach = 1
    while reach < TOK:
        moved = pltpu.roll(scan_a[-1], TOK - reach, 1)
        scan_a.append(scan_a[-1] * jnp.where(time < TOK - reach, moved, 1.0))
        reach *= 2
    slot_lane = lax.broadcasted_iota(jnp.int32, (TOK, SLOTS), 1)
    gathering = (
        (slot_lane == targets[0]).astype(F32) + (slot_lane == targets[1]).astype(F32)
    ).astype(BF16)

    for i in range(1, NSP):
        give(i).wait_recv()
    keep.wait()
    fg[tp] = (cot + dot(gathering, back[...])).astype(BF16)

    def fg_hop(d, k, a):
        o = -k if d == 0 else k
        ref = fg.at[z_at(o) * NC + c, pl.ds(a * (TOK // 2), TOK // 2)]
        return remote(ref, ref, fg_send.at[d, k, a], fg_recv.at[d, k, a], beside[d])

    def fg_mate(o, a):
        ref = fg.at[z_at(o) * NC + c, pl.ds(a * (TOK // 2), TOK // 2)]
        return remote(ref, ref, fgp_send.at[o % NZ, a], fgp_recv.at[o % NZ, a], mate)

    for a in range(2):
        fg_hop(0, 0, a).start()
        fg_hop(1, 0, a).start()
    for a in range(2):
        fg_mate(0, a).start()

    def mixed_grad(o):
        for a in range(2):
            fg_mate(o, a).wait_recv()
        zc = z_at(o)
        cols = pl.ds(pl.multiple_of(zc * 2 * COL, 2 * COL), 2 * COL)
        grads = jnp.concatenate([fg[zc * NC], fg[zc * NC + 1]], axis=1)
        return dot_nt(ow[:, cols], grads)

    d_mixed = None
    for k in range(1, NZ // 2 + 1):
        for a in range(2):
            for d in range(2):
                if k <= REACH[d][a]:
                    fg_hop(d, k - 1, a).wait_recv()
                    if k < REACH[d][a]:
                        fg_hop(d, k, a).start()
                    fg_mate(-k if d == 0 else k, a).start()
        if k == 1:
            d_mixed = mixed_grad(0)
        else:
            d_mixed = d_mixed + mixed_grad(1 - k)
            d_mixed = d_mixed + mixed_grad(k - 1)
    d_mixed = d_mixed + mixed_grad(NZ // 2)

    valve_ref[...] = (d_gelu * (d_mixed * state)).astype(BF16)
    local_sum = d_mixed * gelu
    reach = 1
    for a in scan_a[:-1]:
        moved = pltpu.roll(local_sum, TOK - reach, 1)
        local_sum = local_sum + a * jnp.where(time < TOK - reach, moved, 0.0)
        reach *= 2
    decay_prod = scan_a[-1]
    head_decay = decay[:, 0:1]
    both = jnp.where(lane < HEAD_DIM, head_decay * decay_prod[:, 0:1], head_decay * local_sum[:, 0:1])
    spot = (lane == sub) | (lane == sub + HEAD_DIM)
    row = jnp.sum(jnp.where(spot, both, 0.0), axis=0, keepdims=True)
    summary[...] = jnp.broadcast_to(row, summary.shape)

    def tell(i):
        return remote(summary, summaries.at[s], sum_send.at[i], sum_recv.at[i], peer(i)[1])

    for i in range(1, NSP):
        tell(i).start()

    def piece(i):
        return remote(ow_out.at[i], ow_in.at[i], ow_send.at[i], ow_recv.at[i], peer(i)[1])

    for i in range(1, NSP):
        q, _ = peer(i)
        ow_out[i] = dot(mixed, fg[q]).astype(BF16)
        piece(i).start()
    total = dot(mixed, fg[s]).astype(BF16).astype(F32)

    for i in range(1, NSP):
        tell(i).wait_recv()
    carried = jnp.zeros((1, 2 * HEAD_DIM), F32)
    for q in range(NSP - 1, 0, -1):
        got = summaries[q, 0:1, :]
        stepped = got + pltpu.roll(got, HEAD_DIM, 1) * carried
        carried = jnp.where(q > s, stepped, carried)
    carry = jnp.sum(jnp.where(lane == sub + HEAD_DIM, carried, 0.0), axis=1, keepdims=True)
    state_grad = local_sum + decay_prod * carry
    grad_log = state_grad * prior * decay - state_grad * input_gate * conv * decay * decay / norm
    grad_recur = (grad_log * -RATE_SCALE * softened * recur_gate * (1.0 - recur_gate)).astype(BF16)
    grad_input = (state_grad * norm * conv * input_gate * (1.0 - input_gate)).astype(BF16)
    conv_grad_ref[...] = (
        state_grad * norm * input_gate + dot(w_recur, grad_recur) + dot(w_input, grad_input)
    ).astype(BF16)

    for i in range(1, NSP):
        piece(i).wait_recv()
        total = total + ow_in[i].astype(F32)
    out_grad_ref[...] = total

    for i in range(1, NSP):
        for a in range(2):
            a2a(i, a).wait_send()
        give(i).wait_send()
        tell(i).wait_send()
        piece(i).wait_send()
    for a in range(2):
        for d in range(2):
            for k in range(REACH[d][a]):
                ag_hop(d, k, a).wait_send()
                fg_hop(d, k, a).wait_send()
                rs_hop(d, k, a).wait_send()
        for o in range(NZ):
            ag_mate(o, a).wait_send()
            fg_mate(o, a).wait_send()
            pair_copy(o, a).wait_send()
    store.wait()
    store_acts.wait()


def grads_kernel(chunk, acts, gate_ref, up_ref, down_ref):
    xs = jnp.concatenate([chunk[0, 0], chunk[1, 0]], axis=1)
    cs = jnp.concatenate([chunk[0, 1], chunk[1, 1]], axis=1)
    gate_ref[0] = dot_tn(xs, acts[1]).astype(BF16)
    up_ref[0] = dot_tn(xs, acts[2]).astype(BF16)
    down_ref[0] = dot_tn(acts[0], cs).astype(BF16)


def weight_grads(gathered, acts):
    width = NTP * COL
    return pl.pallas_call(
        grads_kernel,
        grid=(NZ,),
        in_specs=[
            pl.BlockSpec((NC, 2, SLOTS, COL), lambda j: (j, 0, 0, 0)),
            pl.BlockSpec((3, SLOTS, FFD), lambda j: (0, 0, 0)),
        ],
        out_specs=[
            pl.BlockSpec((1, NC * COL, FFD), lambda j: (0, j, 0)),
            pl.BlockSpec((1, NC * COL, FFD), lambda j: (0, j, 0)),
            pl.BlockSpec((1, FFD, NC * COL), lambda j: (0, 0, j)),
        ],
        out_shape=[
            jax.ShapeDtypeStruct((1, width, FFD), BF16),
            jax.ShapeDtypeStruct((1, width, FFD), BF16),
            jax.ShapeDtypeStruct((1, FFD, width), BF16),
        ],
        name="weight_grads",
    )(gathered, acts)


def local(
    cotangent,
    block_input,
    routes,
    route_weights,
    gate_weight,
    up_weight,
    down_weight,
    out_weight,
    conv_out,
    gate_pre,
    prior_states,
    recur_weight,
    input_gate_matrix,
    decay_param,
    decay_jump,
):
    vmem = pl.BlockSpec(memory_space=pltpu.VMEM)
    hbm = pl.BlockSpec(memory_space=pltpu.HBM)
    dma = pltpu.SemaphoreType.DMA
    hops = NZ // 2
    gathered, acts, out_grad, conv_grad, valve = pl.pallas_call(
        main_kernel,
        in_specs=[vmem] * 5 + [hbm] * 10,
        out_specs=[hbm, hbm, vmem, vmem, vmem],
        out_shape=[
            jax.ShapeDtypeStruct((NTP, 2, SLOTS, COL), BF16),
            jax.ShapeDtypeStruct((3, SLOTS, FFD), BF16),
            jax.ShapeDtypeStruct((HEAD_DIM, COL), F32),
            jax.ShapeDtypeStruct((HEAD_DIM, TOK), BF16),
            jax.ShapeDtypeStruct((HEAD_DIM, TOK), BF16),
        ],
        scratch_shapes=[
            pltpu.VMEM((NTP * COL, FFD), BF16),
            pltpu.VMEM((NTP * COL, FFD), BF16),
            pltpu.VMEM((FFD, NTP * COL), BF16),
            pltpu.VMEM((HEAD_DIM, NTP * COL), BF16),
            pltpu.VMEM((HEAD_DIM, TOK), BF16),
            pltpu.VMEM((HEAD_DIM, TOK), BF16),
            pltpu.VMEM((HEAD_DIM, TOK), BF16),
            pltpu.VMEM((HEAD_DIM, TOK), F32),
            pltpu.VMEM((NTP, HEAD_DIM, HEAD_DIM), BF16),
            pltpu.VMEM((NTP, HEAD_DIM, HEAD_DIM), BF16),
            pltpu.VMEM((2, SLOTS, COL), BF16),
            pltpu.VMEM((NTP, 2, SLOTS, COL), BF16),
            pltpu.VMEM((SLOTS, FFD), F32),
            pltpu.VMEM((SLOTS, FFD), F32),
            pltpu.VMEM((SLOTS, FFD), F32),
            pltpu.VMEM((3, SLOTS, FFD), BF16),
            pltpu.VMEM((NZ, SLOTS, COL), F32),
            pltpu.VMEM((NZ, SLOTS, COL), BF16),
            pltpu.VMEM((NZ, SLOTS, COL), BF16),
            pltpu.VMEM((2, hops, 2, HALF, COL), BF16),
            pltpu.VMEM((2, hops, 2, HALF, COL), BF16),
            pltpu.VMEM((SLOTS, COL), BF16),
            pltpu.VMEM((SLOTS, COL), BF16),
            pltpu.VMEM((NTP, TOK, COL), BF16),
            pltpu.VMEM((8, 2 * HEAD_DIM), F32),
            pltpu.VMEM((NSP, 8, 2 * HEAD_DIM), F32),
            pltpu.VMEM((NSP, HEAD_DIM, COL), BF16),
            pltpu.VMEM((NSP, HEAD_DIM, COL), BF16),
            dma((10,)),
            dma((2, NSP)),
            dma((2, NSP)),
            dma((2,)),
            dma((2, hops, 2)),
            dma((2, hops, 2)),
            dma((NZ, 2)),
            dma((NZ, 2)),
            dma((2,)),
            dma((NZ, 2)),
            dma((NZ, 2)),
            dma((2, hops, 2)),
            dma((2, hops, 2)),
            dma((NSP,)),
            dma((NSP,)),
            dma((1,)),
            dma((2, hops, 2)),
            dma((2, hops, 2)),
            dma((NZ, 2)),
            dma((NZ, 2)),
            dma((NSP,)),
            dma((NSP,)),
            dma((NSP,)),
            dma((NSP,)),
        ],
        compiler_params=pltpu.CompilerParams(
            collective_id=0, has_side_effects=True, vmem_limit_bytes=56 * 1024 * 1024
        ),
        name="exchange",
    )(
        routes,
        route_weights,
        block_input,
        cotangent,
        decay_param.reshape(8, 128),
        gate_weight,
        up_weight,
        down_weight,
        out_weight,
        conv_out,
        gate_pre,
        prior_states,
        decay_jump,
        recur_weight,
        input_gate_matrix,
    )
    gate_grad, up_grad, down_grad = weight_grads(gathered, acts)
    return (gate_grad, up_grad, down_grad, out_grad, conv_grad, valve)


def solution(mesh):
    split = Mesh(mesh.devices.reshape(NY, NX, NZ, NC), ("y", "x", "z", "core"))
    sp, tp = ("y", "x"), ("z", "core")
    return jax.shard_map(
        local,
        mesh=split,
        in_specs=(
            P(sp, tp),
            P(sp, tp),
            P(sp, None),
            P(sp, None),
            P(sp, None, tp),
            P(sp, None, tp),
            P(sp, tp, None),
            P(tp, None),
            P(tp, sp),
            P(tp, sp),
            P(tp, sp),
            P(),
            P(),
            P(),
            P(tp, sp),
        ),
        out_specs=(
            P(sp, None, tp),
            P(sp, None, tp),
            P(sp, tp, None),
            P(tp, sp),
            P(tp, sp),
            P(tp, sp),
        ),
        check_vma=False,
    )
```

time: 278 us -> 128 us (0.46)
  waiting for transfers between devices: 141 us -> 0 us
  Pallas kernels: 0 us -> 110 us
  blocking collectives: 29.4 us -> 0 us
  matrix products: 29 us -> 0 us
  local copies, waits for them, and re-layouts: 42 us -> 17.5 us
  between operations: 14.8 us -> 0.66 us
  starting transfers between devices: 10.2 us -> 0 us
  other arithmetic: 10.1 us -> 0 us
    pallas_call x0 -> x2, Pallas kernels: none -> 110 us  [the longest x1 99.5 us: local(): pl.pallas_call(main_kernel, in_specs=[vmem] * 5 + [hbm] * 10, out_specs=[...]
    all_gather x2 -> x0, waiting for transfers between devices: 79.3 us -> none  [the longest x1 54.1 us: side_by_side_2(): whole, at, outs = (lax.all_gather(both, axis, axis=dim, tiled=True), 0, [])]
    reduce_scatter x2 -> x0, waiting for transfers between devices: 53.8 us -> none  [the longest x1 39.3 us: scatter_pairs(): return lax.psum_scatter(tiles, chips, scatter_dimension=0, tiled=True)[0]]
    all_to_all x2 -> x0, blocking collectives: 29.4 us -> none  [the longest x1 15.9 us: side_by_side(): lax.all_to_all(both, axis, split_axis=split_dim, concat_axis=concat_dim,...]
    dot_general x17 -> x0, matrix products: 29 us -> none  [the longest x1 4.89 us: weight_grads(): lax.dot_general(slot_rows, d_gate, major, preferred_element_type=jnp.floa...]
    slice x67 -> x0, local copies, waits for them, and re-layouts: 22.8 us -> none  [the longest x47 19.1 us: local(): lax.associative_scan(link_pairs, (jnp.flip(shifted, 1), jnp.flip(d_state,...]
    unnamed x50 -> x19, local copies, waits for them, and re-layouts: 4.11 us -> 17.5 us
    pad x28 -> x0, local copies, waits for them, and re-layouts: 10.2 us -> none  [local(): lax.associative_scan(link_pairs, (jnp.flip(shifted, 1), jnp.flip(d_state,...]
  transfers between devices with their start and end apart: 6 -> 0, of which waited for: 6 -> 0; matrix products, arithmetic and copies ran while one was open for 7% -> 0% of each run, Pallas kernels for 0% -> 0%
where the time goes in v1:
time: 128 us
  Pallas kernels  110 us (86%)
  local copies, waits for them, and re-layouts  17.5 us (14%)
    pallas_call x1, Pallas kernels, local(): pl.pallas_call(main_kernel, in_specs=[vmem] * 5 + [hbm] * 10, out_specs=[...  99.5 us
    unnamed x19, local copies, waits for them, and re-layouts  17.5 us
    pallas_call x1, Pallas kernels, weight_grads(): pl.pallas_call(grads_kernel, grid=(NZ,), in_specs=[pl.BlockSpec((NC, 2, S...  10.1 us

profile of v1, /device:TPU:1, one launch (start us, length us, event | category | flops | bytes accessed | tf_op | source)
XLA Modules:
  0.0 127.8 jit_solution(12817604079705040097)
XLA Ops:
  0.6 1.5 %copy.21.routes_ref = s32[256,2]{1,0:T(8,128)} copy(s32[256,2]{0,1:T(2,128)} %param.17) | data formatting | bytes 4096 | tf_op args[2]
  2.1 1.5 %copy.22.weights_ref = f32[256,2]{1,0:T(8,128)} copy(f32[256,2]{0,1:T(2,128)} %param.18) | data formatting | bytes 4096 | tf_op args[3]
  3.6 0.0 copy-start.1
  3.6 4.0 %copy.23.gate_hbm = bf16[1,2048,448]{2,1,0:T(8,128)(2,1)} copy(bf16[1,2048,448]{1,2,0:T(8,128)(2,1)} %param.19) | data formatting | bytes 3670016 | tf_op args[4]
  7.5 0.0 copy-done.1
  7.5 2.5 %copy.24.up_hbm = bf16[1,2048,448]{2,1,0:T(8,128)(2,1)} copy(bf16[1,2048,448]{1,2,0:T(8,128)(2,1)S(1)} %copy-done.1) | data formatting | bytes 3670016 | tf_op args[5]
  10.0 99.5 %exchange.1 = (bf16[16,2,640,128]{3,2,1,0:T(8,128)(2,1)}, bf16[3,640,448]{2,1,0:T(8,128)(2,1)}, f32[64,128]{1,0:T(8,128)}, bf16[64,256]{1,0:T(8,128)(2,1)}, bf16[64,256]{1,0:T(8,128)(2,1)}) custom-call(s32[256,2]{1,0:T(8,128)} %copy.21.routes_ref, f32[256,2]{1,0:T(8,128)} %copy.22.weights_ref, bf16[256,128]{1,0:T(8,128)(2,1)} %rows_ref.1, ...), custom_call_target="tpu_custom_call" | custom-call | tf_op jit(solution)/shard_map/exchange/pallas_call | solution.py:575
  109.5 10.1 %weight_grads.1 = (bf16[1,2048,448]{2,1,0:T(8,128)(2,1)}, bf16[1,2048,448]{2,1,0:T(8,128)(2,1)}, bf16[1,448,2048]{2,1,0:T(8,128)(2,1)}) custom-call(bf16[16,2,640,128]{3,2,1,0:T(8,128)(2,1)} %get-tuple-element.14.chunk, bf16[3,640,448]{2,1,0:T(8,128)(2,1)} %get-tuple-element.15.acts), custom_call_target="tpu_custom_call" | custom-call | tf_op jit(solution)/shard_map/weight_grads/pallas_call | solution.py:533
  119.6 0.0 copy-start
  119.6 4.0 %copy.25 = bf16[1,2048,448]{1,2,0:T(8,128)(2,1)} copy(bf16[1,2048,448]{2,1,0:T(8,128)(2,1)} %get-tuple-element.22) | data formatting | bytes 3670016
  123.6 0.0 copy-done
  123.6 0.0 copy-start.4
  123.6 0.0 copy-start.3
  123.6 0.0 copy-start.2
  123.6 2.3 %copy.26 = bf16[1,2048,448]{1,2,0:T(8,128)(2,1)} copy(bf16[1,2048,448]{2,1,0:T(8,128)(2,1)S(1)} %copy-done) | data formatting | bytes 3670016
  125.9 0.0 copy-done.4
  125.9 0.6 copy.30
  126.5 0.0 copy-done.3
  126.5 0.6 copy.31
  127.1 0.0 copy-done.2
  127.1 0.6 copy.32
Async XLA Ops:
  3.6 4.0 %copy-start.1 = (bf16[1,2048,448]{1,2,0:T(8,128)(2,1)S(1)}, bf16[1,2048,448]{1,2,0:T(8,128)(2,1)}, u32[]{:S(2)}) copy-start(bf16[1,2048,448]{1,2,0:T(8,128)(2,1)} %param.20) | copy-start | bytes 5505028
  119.6 4.0 %copy-start = (bf16[1,2048,448]{2,1,0:T(8,128)(2,1)S(1)}, bf16[1,2048,448]{2,1,0:T(8,128)(2,1)}, u32[]{:S(2)}) copy-start(bf16[1,2048,448]{2,1,0:T(8,128)(2,1)} %get-tuple-element.23) | copy-start | bytes 5505028
  123.6 2.3 %copy-start.4 = (f32[64,128]{1,0:T(8,128)S(1)}, f32[64,128]{1,0:T(8,128)}, u32[]{:S(2)}) copy-start(f32[64,128]{1,0:T(8,128)} %get-tuple-element.37) | copy-start | bytes 98308
  123.6 2.9 %copy-start.3 = (bf16[64,256]{1,0:T(8,128)(2,1)S(1)}, bf16[64,256]{1,0:T(8,128)(2,1)}, u32[]{:S(2)}) copy-start(bf16[64,256]{1,0:T(8,128)(2,1)} %get-tuple-element.38) | copy-start | bytes 98308
  123.6 3.5 %copy-start.2 = (bf16[64,256]{1,0:T(8,128)(2,1)S(1)}, bf16[64,256]{1,0:T(8,128)(2,1)}, u32[]{:S(2)}) copy-start(bf16[64,256]{1,0:T(8,128)(2,1)} %get-tuple-element.39) | copy-start | bytes 98308

commit v2 on v1

--- a/solution.py
+++ b/solution.py
@@ -11,6 +11,7 @@
 F32 = jnp.float32
 BF16 = jnp.bfloat16
 MESH = pl.DeviceIdType.MESH
+OUT = pltpu.VMEM
 
 NY, NX, NZ, NC = 4, 4, 8, 2
 NSP = NY * NX
@@ -72,8 +73,9 @@
     jump_hbm,
     recur_hbm,
     input_hbm,
-    gathered_hbm,
-    acts_hbm,
+    gate_out,
+    up_out,
+    down_out,
     out_grad_ref,
     conv_grad_ref,
     valve_ref,
@@ -93,6 +95,7 @@
     acc_u,
     acc_d,
     acts,
+    acts_t,
     own,
     pstage,
     precv,
@@ -113,7 +116,6 @@
     ag_recv,
     agp_send,
     agp_recv,
-    store_sem,
     rp_send,
     rp_recv,
     rr_send,
@@ -170,27 +172,28 @@
     for where in (*beside, mate):
         pl.semaphore_signal(barrier, inc=1, device_id=where, device_id_type=MESH)
 
-    expert_lane = lax.broadcasted_iota(jnp.int32, (TOK, NSP), 1)
-    hot = [(expert_lane == routes_ref[:, k : k + 1]).astype(F32) for k in range(2)]
+    expert_sub = lax.broadcasted_iota(jnp.int32, (NSP, TOK), 0)
+    hot = [(expert_sub == routes_ref[k : k + 1, :]).astype(F32) for k in range(2)]
     tok_sub = lax.broadcasted_iota(jnp.int32, (TOK, TOK), 0)
     tok_lane = lax.broadcasted_iota(jnp.int32, (TOK, TOK), 1)
-    earlier = (tok_lane < tok_sub).astype(BF16)
-    before = dot(earlier, (hot[0] + hot[1]).astype(BF16))
+    before = dot((hot[0] + hot[1]).astype(BF16), (tok_sub < tok_lane).astype(BF16))
     targets = [
-        jnp.sum(hot[k] * before, axis=1, keepdims=True).astype(jnp.int32)
-        + routes_ref[:, k : k + 1] * CAP
+        jnp.sum(hot[k] * before, axis=0, keepdims=True).astype(jnp.int32)
+        + routes_ref[k : k + 1, :] * CAP
         for k in range(2)
     ]
     slot_sub = lax.broadcasted_iota(jnp.int32, (SLOTS, TOK), 0)
-    across = [
-        jnp.sum(jnp.where(tok_sub == tok_lane, t, 0), axis=0, keepdims=True) for t in targets
-    ]
-    hits = [(slot_sub == t).astype(F32) for t in across]
+    hits = [(slot_sub == t).astype(F32) for t in targets]
     placing = (hits[0] + hits[1]).astype(BF16)
+    same = tok_sub == tok_lane
+
+    def upright(row):
+        return jnp.sum(jnp.where(same, row, jnp.zeros_like(row)), axis=1, keepdims=True)
+
     sent[0] = dot(placing, rows_ref[...]).astype(BF16)
     cot = cot_ref[...].astype(F32)
-    sent_cot = dot(hits[0].astype(BF16), (weights_ref[:, 0:1] * cot).astype(BF16)) + dot(
-        hits[1].astype(BF16), (weights_ref[:, 1:2] * cot).astype(BF16)
+    sent_cot = dot(hits[0].astype(BF16), (upright(weights_ref[0:1, :]) * cot).astype(BF16)) + dot(
+        hits[1].astype(BF16), (upright(weights_ref[1:2, :]) * cot).astype(BF16)
     )
     sent[1] = sent_cot.astype(BF16)
 
@@ -245,8 +248,8 @@
             r = pl.ds(pl.multiple_of(m * HALF, HALF), HALF)
             xs = jnp.concatenate([ag[zc * NC, 0, r], ag[zc * NC + 1, 0, r]], axis=1)
             cs = jnp.concatenate([ag[zc * NC, 1, r], ag[zc * NC + 1, 1, r]], axis=1)
-            g = dot(xs, wg[cols, :])
-            u = dot(xs, wu[cols, :])
+            g = dot_nt(xs, wg[:, cols])
+            u = dot_nt(xs, wu[:, cols])
             h = dot_nt(cs, wd[:, cols])
             if first:
                 acc_g[r, :] = g
@@ -275,9 +278,6 @@
             accumulate(k - 1)
     accumulate(NZ // 2)
 
-    store = pltpu.make_async_copy(ag, gathered_hbm, store_sem.at[0])
-    store.start()
-
     def act(m, _):
         r = pl.ds(pl.multiple_of(m * 80, 80), 80)
         g = acc_g[r, :]
@@ -291,9 +291,6 @@
         return 0
 
     lax.fori_loop(0, SLOTS // 80, act, 0)
-    store_acts = pltpu.make_async_copy(acts, acts_hbm, store_sem.at[1])
-    store_acts.start()
-
     def pair_copy(o, a):
         r = pl.ds(a * HALF, HALF)
         return remote(pstage.at[o, r], precv.at[o, r], rp_send.at[o, a], rp_recv.at[o, a], mate)
@@ -302,7 +299,7 @@
         cols = pl.ds(pl.multiple_of(z_at(o) * 2 * COL, 2 * COL), 2 * COL)
         for a in range(2):
             r = pl.ds(a * HALF, HALF)
-            part = dot_nt(acts[1, r, :], wg[cols, :]) + dot_nt(acts[2, r, :], wu[cols, :])
+            part = dot(acts[1, r, :], wg[:, cols]) + dot(acts[2, r, :], wu[:, cols])
             low, high = part[:, :COL], part[:, COL:]
             own[o, r, :] = jnp.where(c == 0, low, high)
             pstage[o, r, :] = jnp.where(c == 0, high, low).astype(BF16)
@@ -330,20 +327,43 @@
         ring_out[d, j, a] = value.astype(BF16)
         rs_hop(d, j, a).start()
 
-    half_way = NZ // 2
-    width(half_way)
-    width(half_way - 1)
-    width(half_way + 1)
-    for j in range(half_way):
+    def turn(i):
+        acts_t[i] = jnp.transpose(acts[i])
+
+    def grads(j):
+        cols = slice(j * 2 * COL, (j + 1) * 2 * COL)
+        xs = jnp.concatenate([ag[2 * j, 0], ag[2 * j + 1, 0]], axis=1)
+        cs = jnp.concatenate([ag[2 * j, 1], ag[2 * j + 1, 1]], axis=1)
+        gate_out[0, :, cols] = dot(acts_t[1], xs).astype(BF16)
+        up_out[0, :, cols] = dot(acts_t[2], xs).astype(BF16)
+        down_out[0, :, cols] = dot(acts_t[0], cs).astype(BF16)
+
+    width(4)
+    width(3)
+    rs_step(0, 0, 0)
+    rs_step(1, 0, 1)
+    width(5)
+    rs_step(0, 0, 1)
+    rs_step(1, 0, 0)
+    width(2)
+    width(6)
+    turn(0)
+    for j in range(1, NZ // 2):
         rs_step(0, j, 0)
         rs_step(1, j, 1)
         rs_step(0, j, 1)
         rs_step(1, j, 0)
-        if j < half_way - 2:
-            width(half_way - 2 - j)
-            width(half_way + 2 + j)
-        if j == half_way - 2:
+        if j == 1:
+            width(1)
+            width(7)
+            turn(1)
+        if j == 2:
             width(0)
+            turn(2)
+            grads(0)
+        if j == 3:
+            grads(1)
+            grads(2)
     for a in range(2):
         r = pl.ds(a * HALF, HALF)
         value = paired(0, a)
@@ -403,9 +423,12 @@
         reach *= 2
     slot_lane = lax.broadcasted_iota(jnp.int32, (TOK, SLOTS), 1)
     gathering = (
-        (slot_lane == targets[0]).astype(F32) + (slot_lane == targets[1]).astype(F32)
+        (slot_lane == upright(targets[0])).astype(F32)
+        + (slot_lane == upright(targets[1])).astype(F32)
     ).astype(BF16)
 
+    grads(3)
+    grads(4)
     for i in range(1, NSP):
         give(i).wait_recv()
     keep.wait()
@@ -443,6 +466,8 @@
                     if k < REACH[d][a]:
                         fg_hop(d, k, a).start()
                     fg_mate(-k if d == 0 else k, a).start()
+        if k < 4:
+            grads(4 + k)
         if k == 1:
             d_mixed = mixed_grad(0)
         else:
@@ -516,39 +541,6 @@
             ag_mate(o, a).wait_send()
             fg_mate(o, a).wait_send()
             pair_copy(o, a).wait_send()
-    store.wait()
-    store_acts.wait()
-
-
-def grads_kernel(chunk, acts, gate_ref, up_ref, down_ref):
-    xs = jnp.concatenate([chunk[0, 0], chunk[1, 0]], axis=1)
-    cs = jnp.concatenate([chunk[0, 1], chunk[1, 1]], axis=1)
-    gate_ref[0] = dot_tn(xs, acts[1]).astype(BF16)
-    up_ref[0] = dot_tn(xs, acts[2]).astype(BF16)
-    down_ref[0] = dot_tn(acts[0], cs).astype(BF16)
-
-
-def weight_grads(gathered, acts):
-    width = NTP * COL
-    return pl.pallas_call(
-        grads_kernel,
-        grid=(NZ,),
-        in_specs=[
-            pl.BlockSpec((NC, 2, SLOTS, COL), lambda j: (j, 0, 0, 0)),
-            pl.BlockSpec((3, SLOTS, FFD), lambda j: (0, 0, 0)),
-        ],
-        out_specs=[
-            pl.BlockSpec((1, NC * COL, FFD), lambda j: (0, j, 0)),
-            pl.BlockSpec((1, NC * COL, FFD), lambda j: (0, j, 0)),
-            pl.BlockSpec((1, FFD, NC * COL), lambda j: (0, 0, j)),
-        ],
-        out_shape=[
-            jax.ShapeDtypeStruct((1, width, FFD), BF16),
-            jax.ShapeDtypeStruct((1, width, FFD), BF16),
-            jax.ShapeDtypeStruct((1, FFD, width), BF16),
-        ],
-        name="weight_grads",
-    )(gathered, acts)
 
 
 def local(
@@ -572,20 +564,21 @@
     hbm = pl.BlockSpec(memory_space=pltpu.HBM)
     dma = pltpu.SemaphoreType.DMA
     hops = NZ // 2
-    gathered, acts, out_grad, conv_grad, valve = pl.pallas_call(
+    gate_grad, up_grad, down_grad, out_grad, conv_grad, valve = pl.pallas_call(
         main_kernel,
         in_specs=[vmem] * 5 + [hbm] * 10,
-        out_specs=[hbm, hbm, vmem, vmem, vmem],
+        out_specs=[vmem] * 6,
         out_shape=[
-            jax.ShapeDtypeStruct((NTP, 2, SLOTS, COL), BF16),
-            jax.ShapeDtypeStruct((3, SLOTS, FFD), BF16),
-            jax.ShapeDtypeStruct((HEAD_DIM, COL), F32),
-            jax.ShapeDtypeStruct((HEAD_DIM, TOK), BF16),
-            jax.ShapeDtypeStruct((HEAD_DIM, TOK), BF16),
+            OUT((1, FFD, NTP * COL), BF16),
+            OUT((1, FFD, NTP * COL), BF16),
+            OUT((1, FFD, NTP * COL), BF16),
+            OUT((HEAD_DIM, COL), F32),
+            OUT((HEAD_DIM, TOK), BF16),
+            OUT((HEAD_DIM, TOK), BF16),
         ],
         scratch_shapes=[
-            pltpu.VMEM((NTP * COL, FFD), BF16),
-            pltpu.VMEM((NTP * COL, FFD), BF16),
+            pltpu.VMEM((FFD, NTP * COL), BF16),
+            pltpu.VMEM((FFD, NTP * COL), BF16),
             pltpu.VMEM((FFD, NTP * COL), BF16),
             pltpu.VMEM((HEAD_DIM, NTP * COL), BF16),
             pltpu.VMEM((HEAD_DIM, TOK), BF16),
@@ -600,6 +593,7 @@
             pltpu.VMEM((SLOTS, FFD), F32),
             pltpu.VMEM((SLOTS, FFD), F32),
             pltpu.VMEM((3, SLOTS, FFD), BF16),
+            pltpu.VMEM((3, FFD, SLOTS), BF16),
             pltpu.VMEM((NZ, SLOTS, COL), F32),
             pltpu.VMEM((NZ, SLOTS, COL), BF16),
             pltpu.VMEM((NZ, SLOTS, COL), BF16),
@@ -620,7 +614,6 @@
             dma((2, hops, 2)),
             dma((NZ, 2)),
             dma((NZ, 2)),
-            dma((2,)),
             dma((NZ, 2)),
             dma((NZ, 2)),
             dma((2, hops, 2)),
@@ -642,13 +635,13 @@
         ),
         name="exchange",
     )(
-        routes,
-        route_weights,
+        routes.T,
+        route_weights.T,
         block_input,
         cotangent,
         decay_param.reshape(8, 128),
-        gate_weight,
-        up_weight,
+        jnp.swapaxes(gate_weight, 1, 2),
+        jnp.swapaxes(up_weight, 1, 2),
         down_weight,
         out_weight,
         conv_out,
@@ -658,8 +651,14 @@
         recur_weight,
         input_gate_matrix,
     )
-    gate_grad, up_grad, down_grad = weight_grads(gathered, acts)
-    return (gate_grad, up_grad, down_grad, out_grad, conv_grad, valve)
+    return (
+        jnp.swapaxes(gate_grad, 1, 2),
+        jnp.swapaxes(up_grad, 1, 2),
+        down_grad,
+        out_grad,
+        conv_grad,
+        valve,
+    )
 
 
 def solution(mesh):

time: 128 us -> 104 us (0.81)
  local copies, waits for them, and re-layouts: 17.5 us -> 5.53 us
  Pallas kernels: 110 us -> 98.1 us
    unnamed x19 -> x6, local copies, waits for them, and re-layouts: 17.5 us -> 5.53 us
    pallas_call x1 -> x0, Pallas kernels: 10.1 us -> none  [weight_grads(): pl.pallas_call(grads_kernel, grid=(NZ,), in_specs=[pl.BlockSpec((NC, 2, S...]
    pallas_call x1, Pallas kernels: 99.5 us -> 98.1 us  [local(): pl.pallas_call(main_kernel, in_specs=[vmem] * 5 + [hbm] * 10, out_specs=[...]
where the time goes in v2:
time: 104 us
  Pallas kernels  98.1 us (94%)
  local copies, waits for them, and re-layouts  5.53 us (5%)
    pallas_call x1, Pallas kernels, local(): pl.pallas_call(main_kernel, in_specs=[vmem] * 5 + [hbm] * 10, out_specs=[...  98.1 us
    unnamed x6, local copies, waits for them, and re-layouts  5.53 us

profile of v2, /device:TPU:1, one launch (start us, length us, event | category | flops | bytes accessed | tf_op | source)
XLA Modules:
  0.0 104.3 jit_solution(9929188603464103467)
XLA Ops:
  0.6 98.1 %exchange.1 = (bf16[1,448,2048]{2,1,0:T(8,128)(2,1)S(1)}, bf16[1,448,2048]{2,1,0:T(8,128)(2,1)S(1)}, bf16[1,448,2048]{2,1,0:T(8,128)(2,1)S(1)}, f32[64,128]{1,0:...) custom-call(s32[2,256]{1,0:T(2,128)} %bitcast.12, f32[2,256]{1,0:T(2,128)} %bitcast.13, ...), custom_call_target="tpu_custom_call" | custom-call | tf_op jit(solution)/shard_map/exchange/pallas_call | solution.py:567
  98.8 1.2 %copy.27 = bf16[1,2048,448]{1,2,0:T(8,128)(2,1)} copy(bf16[1,2048,448]{1,2,0:T(8,128)(2,1)S(1)} %bitcast.8) | data formatting | bytes 3670016
  100.0 1.2 %copy.28 = bf16[1,2048,448]{1,2,0:T(8,128)(2,1)} copy(bf16[1,2048,448]{1,2,0:T(8,128)(2,1)S(1)} %bitcast.7) | data formatting | bytes 3670016
  101.2 0.6 copy.30
  101.8 0.6 copy.31
  102.4 0.6 copy.32
  103.1 1.2 %copy.29 = bf16[1,448,2048]{2,1,0:T(8,128)(2,1)} copy(bf16[1,448,2048]{2,1,0:T(8,128)(2,1)S(1)} %get-tuple-element.20) | data formatting | bytes 3670016

commit v3 on v2

--- a/solution.py
+++ b/solution.py
@@ -90,6 +90,8 @@
     wr,
     wi,
     sent,
+    cots,
+    sent_cot,
     ag,
     acc_g,
     acc_u,
@@ -108,10 +110,17 @@
     summaries,
     ow_out,
     ow_in,
+    grad_buf,
     load_sem,
+    grad_sem,
     a2a_send,
     a2a_recv,
     a2a_self,
+    cg_send,
+    cg_recv,
+    cd_send,
+    cd_recv,
+    cd_self,
     ag_send,
     ag_recv,
     agp_send,
@@ -190,93 +199,206 @@
     def upright(row):
         return jnp.sum(jnp.where(same, row, jnp.zeros_like(row)), axis=1, keepdims=True)
 
-    sent[0] = dot(placing, rows_ref[...]).astype(BF16)
+    slot_weight = jnp.sum(
+        hits[0] * weights_ref[0:1, :] + hits[1] * weights_ref[1:2, :], axis=1, keepdims=True
+    )
     cot = cot_ref[...].astype(F32)
-    sent_cot = dot(hits[0].astype(BF16), (upright(weights_ref[0:1, :]) * cot).astype(BF16)) + dot(
-        hits[1].astype(BF16), (upright(weights_ref[1:2, :]) * cot).astype(BF16)
-    )
-    sent[1] = sent_cot.astype(BF16)
 
     pl.semaphore_wait(barrier, NSP - 1 + 3)
 
-    def a2a(i, a):
+    def cot_hop(d, k, a):
+        o = -k if d == 0 else k
+        part = pl.ds(a * (TOK // 2), TOK // 2)
+        there = cots.at[z_at(o), part]
+        here = cot_ref.at[part] if k == 0 else there
+        return remote(here, there, cg_send.at[d, k, a], cg_recv.at[d, k, a], beside[d])
+
+    for a in range(2):
+        for d in range(2):
+            cot_hop(d, 0, a).start()
+
+    mine = pl.ds(pl.multiple_of(s * CAP, 8), CAP)
+
+    def a2a(i):
         q, where = peer(i)
         return remote(
-            sent.at[a, pl.ds(pl.multiple_of(q * CAP, 8), CAP)],
-            ag.at[tp, a, pl.ds(pl.multiple_of(s * CAP, 8), CAP)],
-            a2a_send.at[a, i],
-            a2a_recv.at[a, i],
+            sent.at[pl.ds(pl.multiple_of(q * CAP, 8), CAP)],
+            ag.at[tp, 0, mine],
+            a2a_send.at[i],
+            a2a_recv.at[i],
             where,
         )
 
-    selfs = []
-    for a in range(2):
-        for i in range(1, NSP):
-            a2a(i, a).start()
-        mine = pl.ds(pl.multiple_of(s * CAP, 8), CAP)
-        selfs.append(pltpu.make_async_copy(sent.at[a, mine], ag.at[tp, a, mine], a2a_self.at[a]))
-        selfs[-1].start()
+    first = dot(placing, jnp.concatenate([rows_ref[...], cot_ref[...]], axis=1))
+    sent[...] = first[:, :COL].astype(BF16)
+    for i in range(1, NSP):
+        a2a(i).start()
+    rows_self = pltpu.make_async_copy(sent.at[mine], ag.at[tp, 0, mine], a2a_self.at[0])
+    rows_self.start()
+
+    def cot_copy(o, i):
+        q, where = peer(i)
+        zc = z_at(o)
+        return remote(
+            sent_cot.at[zc, pl.ds(pl.multiple_of(q * CAP, 8), CAP)],
+            ag.at[zc * NC + c, 1, mine],
+            cd_send.at[o % NZ, i],
+            cd_recv.at[o % NZ, i],
+            where,
+        )
+
+    def cot_self(o):
+        zc = z_at(o)
+        return pltpu.make_async_copy(
+            sent_cot.at[zc, mine], ag.at[zc * NC + c, 1, mine], cd_self.at[o % NZ]
+        )
+
+    def send_cot(*offsets):
+        if offsets == (0,):
+            placed = first[:, COL:]
+        else:
+            placed = dot(placing, jnp.concatenate([cots[z_at(o)] for o in offsets], axis=1))
+        placed = (slot_weight * placed).astype(BF16)
+        for n, o in enumerate(offsets):
+            sent_cot[z_at(o)] = placed[:, n * COL : (n + 1) * COL]
+        for o in offsets:
+            cot_self(o).start()
+
+            def one(i, _, o=o):
+                cot_copy(o, i).start()
+                return 0
+
+            lax.fori_loop(1, NSP, one, 0)
+
+    def got_cot(o):
+        def one(i, _):
+            cot_copy(o, i).wait_recv()
+            return 0
+
+        lax.fori_loop(1, NSP, one, 0)
+        cot_self(o).wait()
+        ag_mate(o, 1, 0).start()
+        ag_mate(o, 1, 1).start()
 
     def ag_hop(d, k, a):
         o = -k if d == 0 else k
-        ref = ag.at[z_at(o) * NC + c, a]
+        ref = ag.at[z_at(o) * NC + c, 0, pl.ds(a * HALF, HALF)]
         return remote(ref, ref, ag_send.at[d, k, a], ag_recv.at[d, k, a], beside[d])
 
-    def ag_mate(o, a):
-        ref = ag.at[z_at(o) * NC + c, a]
-        return remote(ref, ref, agp_send.at[o % NZ, a], agp_recv.at[o % NZ, a], mate)
-
+    def ag_mate(o, b, a):
+        ref = ag.at[z_at(o) * NC + c, b, pl.ds(a * HALF, HALF)]
+        return remote(ref, ref, agp_send.at[o % NZ, b, a], agp_recv.at[o % NZ, b, a], mate)
+
+    def cot_step(k):
+        for a in range(2):
+            for d in range(2):
+                if k <= REACH[d][a]:
+                    cot_hop(d, k - 1, a).wait_recv()
+                    if k < REACH[d][a]:
+                        cot_hop(d, k, a).start()
+
+    def rows_step(k, a):
+        for d in range(2):
+            if k <= REACH[d][a]:
+                ag_hop(d, k - 1, a).wait_recv()
+                if k < REACH[d][a]:
+                    ag_hop(d, k, a).start()
+                ag_mate(-k if d == 0 else k, 0, a).start()
+
+    def columns(o):
+        return pl.ds(pl.multiple_of(z_at(o) * 2 * COL, 2 * COL), 2 * COL)
+
+    def add_rows(o):
+        for a in range(2):
+            ag_mate(o, 0, a).wait_recv()
+        zc = z_at(o)
+        cols = columns(o)
+
+        def block(m, _):
+            r = pl.ds(pl.multiple_of(m * HALF, HALF), HALF)
+            xs = jnp.concatenate([ag[zc * NC, 0, r], ag[zc * NC + 1, 0, r]], axis=1)
+            g = dot_nt(xs, wg[:, cols])
+            u = dot_nt(xs, wu[:, cols])
+            if o == 0:
+                acc_g[r, :] = g
+                acc_u[r, :] = u
+            else:
+                acc_g[r, :] += g
+                acc_u[r, :] += u
+            return 0
+
+        lax.fori_loop(0, 2, block, 0)
+
+    def add_cot(o):
+        for a in range(2):
+            ag_mate(o, 1, a).wait_recv()
+        zc = z_at(o)
+        cols = columns(o)
+
+        def block(m, _):
+            r = pl.ds(pl.multiple_of(m * HALF, HALF), HALF)
+            cs = jnp.concatenate([ag[zc * NC, 1, r], ag[zc * NC + 1, 1, r]], axis=1)
+            h = dot_nt(cs, wd[:, cols])
+            if o == 0:
+                acc_d[r, :] = h
+            else:
+                acc_d[r, :] += h
+            return 0
+
+        lax.fori_loop(0, 2, block, 0)
+
+    send_cot(0)
+    cot_step(1)
+    send_cot(-1, 1)
+    for i in range(1, NSP):
+        a2a(i).wait_recv()
+    rows_self.wait()
+    for a in range(2):
+        ag_hop(0, 0, a).start()
+        ag_hop(1, 0, a).start()
+    for a in range(2):
+        ag_mate(0, 0, a).start()
+    cot_step(2)
+    send_cot(-2, 2)
+    rows_step(1, 0)
+    cot_step(3)
+    rows_step(1, 1)
+    send_cot(-3, 3)
+    cot_step(4)
+    send_cot(4)
     loads[0].wait()
     loads[1].wait()
     loads[2].wait()
-
-    for a in range(2):
-        for i in range(1, NSP):
-            a2a(i, a).wait_recv()
-        selfs[a].wait()
-        ag_hop(0, 0, a).start()
-        ag_hop(1, 0, a).start()
-        ag_mate(0, a).start()
-
-    def accumulate(o, first=False):
-        for a in range(2):
-            ag_mate(o, a).wait_recv()
-        zc = z_at(o)
-        cols = pl.ds(pl.multiple_of(zc * 2 * COL, 2 * COL), 2 * COL)
-
-        def block(m, _):
-            r = pl.ds(pl.multiple_of(m * HALF, HALF), HALF)
-            xs = jnp.concatenate([ag[zc * NC, 0, r], ag[zc * NC + 1, 0, r]], axis=1)
-            cs = jnp.concatenate([ag[zc * NC, 1, r], ag[zc * NC + 1, 1, r]], axis=1)
-            g = dot_nt(xs, wg[:, cols])
-            u = dot_nt(xs, wu[:, cols])
-            h = dot_nt(cs, wd[:, cols])
-            if first:
-                acc_g[r, :] = g
-                acc_u[r, :] = u
-                acc_d[r, :] = h
-            else:
-                acc_g[r, :] += g
-                acc_u[r, :] += u
-                acc_d[r, :] += h
-            return 0
-
-        lax.fori_loop(0, 2, block, 0)
-
-    for k in range(1, NZ // 2 + 1):
-        for a in range(2):
-            for d in range(2):
-                if k <= REACH[d][a]:
-                    ag_hop(d, k - 1, a).wait_recv()
-                    if k < REACH[d][a]:
-                        ag_hop(d, k, a).start()
-                    ag_mate(-k if d == 0 else k, a).start()
-        if k == 1:
-            accumulate(0, True)
-        else:
-            accumulate(1 - k)
-            accumulate(k - 1)
-    accumulate(NZ // 2)
+    rows_step(2, 0)
+    add_rows(0)
+    got_cot(0)
+    rows_step(2, 1)
+    add_cot(0)
+    got_cot(-1)
+    got_cot(1)
+    add_rows(-1)
+    add_cot(-1)
+    add_cot(1)
+    got_cot(-2)
+    got_cot(2)
+    rows_step(3, 0)
+    add_rows(1)
+    add_cot(-2)
+    rows_step(3, 1)
+    add_cot(2)
+    got_cot(-3)
+    got_cot(3)
+    add_rows(-2)
+    add_rows(2)
+    rows_step(4, 0)
+    got_cot(4)
+    add_cot(-3)
+    add_cot(3)
+    add_rows(-3)
+    rows_step(4, 1)
+    add_cot(4)
+    add_rows(3)
+    add_rows(4)
 
     def act(m, _):
         r = pl.ds(pl.multiple_of(m * 80, 80), 80)
@@ -290,20 +412,18 @@
         acts[2, r, :] = (dh * silu).astype(BF16)
         return 0
 
-    lax.fori_loop(0, SLOTS // 80, act, 0)
     def pair_copy(o, a):
         r = pl.ds(a * HALF, HALF)
         return remote(pstage.at[o, r], precv.at[o, r], rp_send.at[o, a], rp_recv.at[o, a], mate)
 
-    def width(o):
-        cols = pl.ds(pl.multiple_of(z_at(o) * 2 * COL, 2 * COL), 2 * COL)
-        for a in range(2):
-            r = pl.ds(a * HALF, HALF)
-            part = dot(acts[1, r, :], wg[:, cols]) + dot(acts[2, r, :], wu[:, cols])
-            low, high = part[:, :COL], part[:, COL:]
-            own[o, r, :] = jnp.where(c == 0, low, high)
-            pstage[o, r, :] = jnp.where(c == 0, high, low).astype(BF16)
-            pair_copy(o, a).start()
+    def width(o, a):
+        cols = columns(o)
+        r = pl.ds(a * HALF, HALF)
+        part = dot(acts[1, r, :], wg[:, cols]) + dot(acts[2, r, :], wu[:, cols])
+        low, high = part[:, :COL], part[:, COL:]
+        own[o, r, :] = jnp.where(c == 0, low, high)
+        pstage[o, r, :] = jnp.where(c == 0, high, low).astype(BF16)
+        pair_copy(o, a).start()
 
     def paired(o, a):
         pair_copy(o, a).wait_recv()
@@ -334,36 +454,48 @@
         cols = slice(j * 2 * COL, (j + 1) * 2 * COL)
         xs = jnp.concatenate([ag[2 * j, 0], ag[2 * j + 1, 0]], axis=1)
         cs = jnp.concatenate([ag[2 * j, 1], ag[2 * j + 1, 1]], axis=1)
-        gate_out[0, :, cols] = dot(acts_t[1], xs).astype(BF16)
-        up_out[0, :, cols] = dot(acts_t[2], xs).astype(BF16)
-        down_out[0, :, cols] = dot(acts_t[0], cs).astype(BF16)
-
-    width(4)
-    width(3)
+        grad_buf[0, :, cols] = dot(acts_t[1], xs).astype(BF16)
+        grad_buf[1, :, cols] = dot(acts_t[2], xs).astype(BF16)
+        grad_buf[2, :, cols] = dot(acts_t[0], cs).astype(BF16)
+        for i in range(3):
+            grad_copy(j, i).start()
+
+    def grad_copy(j, i):
+        cols = pl.ds(j * 2 * COL, 2 * COL)
+        out = (gate_out, up_out, down_out)[i]
+        return pltpu.make_async_copy(grad_buf.at[i, :, cols], out.at[0, :, cols], grad_sem.at[j, i])
+
+    for a in range(2):
+        lax.fori_loop(a * (HALF // 80), (a + 1) * (HALF // 80), act, 0)
+        width(4, a)
     rs_step(0, 0, 0)
+    width(3, 1)
     rs_step(1, 0, 1)
-    width(5)
+    width(5, 0)
     rs_step(0, 0, 1)
+    width(3, 0)
     rs_step(1, 0, 0)
-    width(2)
-    width(6)
-    turn(0)
+    width(5, 1)
+    width(2, 1)
+    width(6, 0)
     for j in range(1, NZ // 2):
         rs_step(0, j, 0)
         rs_step(1, j, 1)
         rs_step(0, j, 1)
         rs_step(1, j, 0)
         if j == 1:
-            width(1)
-            width(7)
-            turn(1)
+            width(2, 0)
+            width(6, 1)
+            width(1, 1)
+            width(7, 0)
         if j == 2:
-            width(0)
-            turn(2)
-            grads(0)
+            width(1, 0)
+            width(7, 1)
+            width(0, 0)
+            width(0, 1)
         if j == 3:
-            grads(1)
-            grads(2)
+            for i in range(3):
+                turn(i)
     for a in range(2):
         r = pl.ds(a * HALF, HALF)
         value = paired(0, a)
@@ -385,7 +517,6 @@
 
     for i in range(1, NSP):
         give(i).start()
-    mine = pl.ds(pl.multiple_of(s * CAP, 8), CAP)
     keep = pltpu.make_async_copy(sums.at[mine], back.at[mine], back_self.at[0])
     keep.start()
 
@@ -427,8 +558,8 @@
         + (slot_lane == upright(targets[1])).astype(F32)
     ).astype(BF16)
 
-    grads(3)
-    grads(4)
+    for j in range(4):
+        grads(j)
     for i in range(1, NSP):
         give(i).wait_recv()
     keep.wait()
@@ -436,43 +567,61 @@
 
     def fg_hop(d, k, a):
         o = -k if d == 0 else k
-        ref = fg.at[z_at(o) * NC + c, pl.ds(a * (TOK // 2), TOK // 2)]
+        ref = fg.at[z_at(o) * NC + c, pl.ds(a * (TOK // 4), TOK // 4)]
         return remote(ref, ref, fg_send.at[d, k, a], fg_recv.at[d, k, a], beside[d])
 
     def fg_mate(o, a):
-        ref = fg.at[z_at(o) * NC + c, pl.ds(a * (TOK // 2), TOK // 2)]
+        ref = fg.at[z_at(o) * NC + c, pl.ds(a * (TOK // 4), TOK // 4)]
         return remote(ref, ref, fgp_send.at[o % NZ, a], fgp_recv.at[o % NZ, a], mate)
 
-    for a in range(2):
+    for a in range(4):
         fg_hop(0, 0, a).start()
         fg_hop(1, 0, a).start()
-    for a in range(2):
+    for a in range(4):
         fg_mate(0, a).start()
 
+    def piece(i):
+        return remote(ow_out.at[i], ow_in.at[i], ow_send.at[i], ow_recv.at[i], peer(i)[1])
+
+    def pieces(o):
+        zc = z_at(o)
+        both = jnp.concatenate([fg[zc * NC], fg[zc * NC + 1]], axis=1)
+        found = dot(mixed, both).astype(BF16)
+        for h in range(NC):
+            i = lax.rem(zc * NC + h + NSP - s, NSP)
+            ow_out[i] = found[:, h * COL : (h + 1) * COL]
+
+            @pl.when(i != 0)
+            def _():
+                piece(i).start()
+
     def mixed_grad(o):
-        for a in range(2):
+        for a in range(4):
             fg_mate(o, a).wait_recv()
         zc = z_at(o)
-        cols = pl.ds(pl.multiple_of(zc * 2 * COL, 2 * COL), 2 * COL)
-        grads = jnp.concatenate([fg[zc * NC], fg[zc * NC + 1]], axis=1)
-        return dot_nt(ow[:, cols], grads)
+        both = jnp.concatenate([fg[zc * NC], fg[zc * NC + 1]], axis=1)
+        return dot_nt(ow[:, columns(o)], both)
 
     d_mixed = None
     for k in range(1, NZ // 2 + 1):
-        for a in range(2):
+        for a in range(4):
             for d in range(2):
-                if k <= REACH[d][a]:
+                if k <= REACH[d][a // 2]:
                     fg_hop(d, k - 1, a).wait_recv()
-                    if k < REACH[d][a]:
+                    if k < REACH[d][a // 2]:
                         fg_hop(d, k, a).start()
                     fg_mate(-k if d == 0 else k, a).start()
-        if k < 4:
-            grads(4 + k)
+        if k < 3:
+            grads(3 + k)
         if k == 1:
             d_mixed = mixed_grad(0)
+            pieces(0)
         else:
             d_mixed = d_mixed + mixed_grad(1 - k)
             d_mixed = d_mixed + mixed_grad(k - 1)
+            if k < 4:
+                pieces(1 - k)
+                pieces(k - 1)
     d_mixed = d_mixed + mixed_grad(NZ // 2)
 
     valve_ref[...] = (d_gelu * (d_mixed * state)).astype(BF16)
@@ -494,15 +643,10 @@
 
     for i in range(1, NSP):
         tell(i).start()
-
-    def piece(i):
-        return remote(ow_out.at[i], ow_in.at[i], ow_send.at[i], ow_recv.at[i], peer(i)[1])
-
-    for i in range(1, NSP):
-        q, _ = peer(i)
-        ow_out[i] = dot(mixed, fg[q]).astype(BF16)
-        piece(i).start()
-    total = dot(mixed, fg[s]).astype(BF16).astype(F32)
+    for o in (-3, 3, 4):
+        pieces(o)
+    grads(6)
+    grads(7)
 
     for i in range(1, NSP):
         tell(i).wait_recv()
@@ -520,27 +664,61 @@
         state_grad * norm * input_gate + dot(w_recur, grad_recur) + dot(w_input, grad_input)
     ).astype(BF16)
 
+    total = ow_out[0].astype(F32)
     for i in range(1, NSP):
         piece(i).wait_recv()
         total = total + ow_in[i].astype(F32)
     out_grad_ref[...] = total
 
+    for j in range(NZ):
+        for i in range(3):
+            grad_copy(j, i).wait()
     for i in range(1, NSP):
-        for a in range(2):
-            a2a(i, a).wait_send()
+        a2a(i).wait_send()
         give(i).wait_send()
         tell(i).wait_send()
         piece(i).wait_send()
+    def left(i, _):
+        for o in range(NZ):
+            cot_copy(o, i).wait_send()
+        return 0
+
+    lax.fori_loop(1, NSP, left, 0)
     for a in range(2):
         for d in range(2):
             for k in range(REACH[d][a]):
                 ag_hop(d, k, a).wait_send()
-                fg_hop(d, k, a).wait_send()
+                cot_hop(d, k, a).wait_send()
+                fg_hop(d, k, 2 * a).wait_send()
+                fg_hop(d, k, 2 * a + 1).wait_send()
                 rs_hop(d, k, a).wait_send()
         for o in range(NZ):
-            ag_mate(o, a).wait_send()
-            fg_mate(o, a).wait_send()
+            ag_mate(o, 0, a).wait_send()
+            ag_mate(o, 1, a).wait_send()
+            fg_mate(o, 2 * a).wait_send()
+            fg_mate(o, 2 * a + 1).wait_send()
             pair_copy(o, a).wait_send()
+
+
+def write_kernel(*refs):
+    sources, targets, sem = refs[:6], refs[6:12], refs[12]
+    copies = [pltpu.make_async_copy(a, b, sem.at[i]) for i, (a, b) in enumerate(zip(sources, targets))]
+    for copy in copies:
+        copy.start()
+    for copy in copies:
+        copy.wait()
+
+
+def written(results):
+    return pl.pallas_call(
+        write_kernel,
+        in_specs=[pl.BlockSpec(memory_space=pl.ANY)] * 6,
+        out_specs=[pl.BlockSpec(memory_space=pltpu.HBM)] * 6,
+        out_shape=[jax.ShapeDtypeStruct(r.shape, r.dtype) for r in results],
+        scratch_shapes=[pltpu.SemaphoreType.DMA((6,))],
+        compiler_params=pltpu.CompilerParams(vmem_limit_bytes=1024 * 1024),
+        name="write",
+    )(*results)
 
 
 def local(
@@ -564,10 +742,10 @@
     hbm = pl.BlockSpec(memory_space=pltpu.HBM)
     dma = pltpu.SemaphoreType.DMA
     hops = NZ // 2
-    gate_grad, up_grad, down_grad, out_grad, conv_grad, valve = pl.pallas_call(
+    results = pl.pallas_call(
         main_kernel,
         in_specs=[vmem] * 5 + [hbm] * 10,
-        out_specs=[vmem] * 6,
+        out_specs=[pl.BlockSpec(memory_space=pl.ANY)] * 3 + [vmem] * 3,
         out_shape=[
             OUT((1, FFD, NTP * COL), BF16),
             OUT((1, FFD, NTP * COL), BF16),
@@ -587,7 +765,9 @@
             pltpu.VMEM((HEAD_DIM, TOK), F32),
             pltpu.VMEM((NTP, HEAD_DIM, HEAD_DIM), BF16),
             pltpu.VMEM((NTP, HEAD_DIM, HEAD_DIM), BF16),
-            pltpu.VMEM((2, SLOTS, COL), BF16),
+            pltpu.VMEM((SLOTS, COL), BF16),
+            pltpu.VMEM((NZ, TOK, COL), BF16),
+            pltpu.VMEM((NZ, SLOTS, COL), BF16),
             pltpu.VMEM((NTP, 2, SLOTS, COL), BF16),
             pltpu.VMEM((SLOTS, FFD), F32),
             pltpu.VMEM((SLOTS, FFD), F32),
@@ -606,14 +786,21 @@
             pltpu.VMEM((NSP, 8, 2 * HEAD_DIM), F32),
             pltpu.VMEM((NSP, HEAD_DIM, COL), BF16),
             pltpu.VMEM((NSP, HEAD_DIM, COL), BF16),
+            pltpu.VMEM((3, FFD, NTP * COL), BF16),
             dma((10,)),
-            dma((2, NSP)),
-            dma((2, NSP)),
-            dma((2,)),
+            dma((NZ, 3)),
+            dma((NSP,)),
+            dma((NSP,)),
+            dma((1,)),
             dma((2, hops, 2)),
             dma((2, hops, 2)),
-            dma((NZ, 2)),
-            dma((NZ, 2)),
+            dma((NZ, NSP)),
+            dma((NZ, NSP)),
+            dma((NZ,)),
+            dma((2, hops, 2)),
+            dma((2, hops, 2)),
+            dma((NZ, 2, 2)),
+            dma((NZ, 2, 2)),
             dma((NZ, 2)),
             dma((NZ, 2)),
             dma((2, hops, 2)),
@@ -621,17 +808,17 @@
             dma((NSP,)),
             dma((NSP,)),
             dma((1,)),
-            dma((2, hops, 2)),
-            dma((2, hops, 2)),
-            dma((NZ, 2)),
-            dma((NZ, 2)),
+            dma((2, hops, 4)),
+            dma((2, hops, 4)),
+            dma((NZ, 4)),
+            dma((NZ, 4)),
             dma((NSP,)),
             dma((NSP,)),
             dma((NSP,)),
             dma((NSP,)),
         ],
         compiler_params=pltpu.CompilerParams(
-            collective_id=0, has_side_effects=True, vmem_limit_bytes=56 * 1024 * 1024
+            collective_id=0, has_side_effects=True, vmem_limit_bytes=57 * 1024 * 1024
         ),
         name="exchange",
     )(
@@ -651,6 +838,7 @@
         recur_weight,
         input_gate_matrix,
     )
+    gate_grad, up_grad, down_grad, out_grad, conv_grad, valve = written(results)
     return (
         jnp.swapaxes(gate_grad, 1, 2),
         jnp.swapaxes(up_grad, 1, 2),

time: 104 us -> 97.6 us (0.938)
  local copies, waits for them, and re-layouts: 5.53 us -> 0 us
  Pallas kernels: 98.1 us -> 96.7 us
    unnamed x6 -> x0, local copies, waits for them, and re-layouts: 5.53 us -> none
    pallas_call x1, Pallas kernels: 98.1 us -> 94.2 us  [local(): pl.pallas_call(main_kernel, in_specs=[vmem] * 5 + [hbm] * 10, out_specs=[...]
    pallas_call x0 -> x1, Pallas kernels: none -> 2.5 us  [written(): pl.pallas_call(write_kernel, in_specs=[pl.BlockSpec(memory_space=pl.ANY)]...]
where the time goes in v3:
time: 97.6 us; the launch traced here: 97.5 us
  Pallas kernels  96.7 us (99%)
    pallas_call x1, Pallas kernels, local(): pl.pallas_call(main_kernel, in_specs=[vmem] * 5 + [hbm] * 10, out_specs=[...  94.2 us
    pallas_call x1, Pallas kernels, written(): pl.pallas_call(write_kernel, in_specs=[pl.BlockSpec(memory_space=pl.ANY)]...  2.5 us

profile of v3, /device:TPU:1, one launch (start us, length us, event | category | flops | bytes accessed | tf_op | source)
XLA Modules:
  0.0 97.5 jit_solution(14119225499140793663)
XLA Ops:
  0.6 94.2 %exchange.1 = (bf16[1,448,2048]{2,1,0:T(8,128)(2,1)S(1)}, bf16[1,448,2048]{2,1,0:T(8,128)(2,1)S(1)}, bf16[1,448,2048]{2,1,0:T(8,128)(2,1)S(1)}, f32[64,128]{1,0:...) custom-call(s32[2,256]{1,0:T(2,128)} %bitcast.10, f32[2,256]{1,0:T(2,128)} %bitcast.11, ...), custom_call_target="tpu_custom_call" | custom-call | tf_op jit(solution)/shard_map/exchange/pallas_call | solution.py:745
  94.8 2.5 %write.1 = (bf16[1,448,2048]{2,1,0:T(8,128)(2,1)}, bf16[1,448,2048]{2,1,0:T(8,128)(2,1)}, bf16[1,448,2048]{2,1,0:T(8,128)(2,1)}, f32[64,128]{1,0:T(8,128)}, bf16...) custom-call(bf16[1,448,2048]{2,1,0:T(8,128)(2,1)S(1)} %get-tuple-element.18.refs_0_, ...), custom_call_target="tpu_custom_call" | custom-call | tf_op jit(solution)/shard_map/write/pallas_call | solution.py:713
